TPU v7x, 512 devices: a whole 4x4x16 slice. The times are simulated.
512 devices in a mesh: sp: 32 (over z, core), tp: 16 (over y, x).
Axes of the slice: x: 4, y: 4, z: 16, core: 2. Of those that a mesh axis runs over, the one named last changes fastest.
Arguments:
- skip_path_vectors: bfloat16 [8192, 2048], P('sp'), may hold values from -10 to 10
- asker_raw_scores: bfloat16 [8192, 2048], P('sp', 'tp'), may hold values from -6 to 6
- retain_raw_scores: bfloat16 [8192, 2048], P('sp', 'tp'), may hold values from -5.5 to 5.5
- memory_write_entries: bfloat16 [8192, 2048], P('sp', 'tp'), may hold values from -6 to 6
- emit_switch_scores: bfloat16 [8192, 2048], P('sp', 'tp'), may hold values from -6 to 6
- retain_minimum_share: float32 [2048], P('tp'), may hold values from 0.88 to 0.99997559
- extra_shrink_rate: float32 [16, 8192], P('tp', 'sp'), may hold values from -0.7 to 0
- lane_rescale_factor: float32 [128], replicated, may hold values from 0.1 to 1.9
- emit_projection_array: bfloat16 [2048, 2048], P('tp'), may hold values from -0.1875 to 0.1875
- specialist_rescale_factor: float32 [2048], replicated, may hold values from 0.1 to 1.9
- specialist_switch_proj: bfloat16 [32, 2048, 4096], P('sp', None, 'tp'), may hold values from -0.125 to 0.125
- specialist_raise_proj: bfloat16 [32, 2048, 4096], P('sp', None, 'tp'), may hold values from -0.125 to 0.125
- specialist_lower_proj: bfloat16 [32, 4096, 2048], P('sp', 'tp'), may hold values from -0.375 to 0.375
- specialist_choice_ids: int32 [8192, 2], P('sp'), may hold values from 0 to 31, all different within a row; in each aligned block of 256 rows (0 to 255, 256 to 511, ...) at most 24 rows name the same one
- cluster_chance: float32 [8192], P('sp'), may hold values from 0.1 to 0.6
- specialist_duo_scores: float32 [8192, 2], P('sp'), may hold values from -2 to 2
Outputs:
- mixed_out: bfloat16 [8192, 2048], P('sp', 'tp')
Inputs may be any that keep to these rules, and one draw needn't show every extreme that they name: `specialist_choice_ids`: in each aligned block of 256 rows (the rows of one index of sp) no expert is named by more than 24 rows, a bound that some block reaches; the 2 ids of a row differ.
All inputs are finite; a program needn't handle non-finite values.
Results may differ from a plain program's by a relative error of at most 0.02.
Values may be sent and summed in bfloat16 or wider, within the bound.
A program may use at most 64 MiB of HBM per device.

v0:
```python
import functools

import jax
import jax.numpy as jnp
from jax import lax
from jax.sharding import Mesh
from jax.sharding import PartitionSpec as P

SP = ("sp_0", "sp_1")
TP = ("tp_0", "tp_1")


EPS = 1e-06
PRECISE = lax.Precision.HIGHEST


def filled_with(array, identity):
    return jax.tree.map(
        lambda a, e: jnp.broadcast_to(jnp.asarray(e, a.dtype), a.shape), array, identity
    )


def gathered_once(array, axis):
    leaves = jax.tree.leaves(array)
    turns = sorted(range(len(leaves)), key=lambda k: -leaves[k].size)
    width = (1, *leaves[turns[0]].shape)[-1]
    lines = [
        jnp.pad(leaves[k].reshape(-1), (0, -leaves[k].size % width)).reshape(-1, width)
        for k in turns
    ]
    both, at, found = (lax.all_gather(jnp.concatenate(lines), axis), 0, {})
    for k, line in zip(turns, lines):
        section = both[:, at : at + len(line)].reshape(len(both), -1)
        found[k] = section[:, : leaves[k].size].reshape(-1, *leaves[k].shape)
        at += len(line)
    numbers = iter(range(len(leaves)))
    return jax.tree.map(lambda _: found[next(numbers)], array)


def prefix_by_axis(array, axes, combine, identity):
    before = start = filled_with(array, identity)
    total = array
    for axis in reversed(axes):
        count, position = (lax.axis_size(axis), lax.axis_index(axis))
        pieces = gathered_once(
            jax.tree.map(lambda part, kind: part.astype(kind), total, (jnp.bfloat16, jnp.bfloat16)),
            axis,
        )
        inside, total = (start, start)
        for k in range(count):
            passed = k < position
            total = combine(
                total, jax.tree.map(lambda part, own: part[k].astype(own.dtype), pieces, array)
            )
            inside = jax.tree.map(lambda new, old: jnp.where(passed, new, old), total, inside)
        before = combine(inside, before)
    return before


def cut_along(array, dim, count):
    before, after = (array.shape[:dim], array.shape[dim + 1 :])
    return jnp.moveaxis(array.reshape(*before, count, -1, *after), dim, 0)


def sent_and_summed(array, axis, dim):
    count = lax.axis_size(axis)
    parts = lax.all_to_all(cut_along(array, dim, count), axis, 0, 0, tiled=True)
    return jnp.sum(parts.astype(jnp.float32), axis=0)


def over_axes(array, axes):
    return functools.reduce(lax.psum, axes, array)


def whole_of(array, axes, dim):
    if not axes:
        return array
    nearer = lax.all_gather(array, axes[-1], axis=dim, tiled=True)
    return whole_of(nearer, axes[:-1], dim)


def chain_join(earlier, later):
    return (earlier[0] * later[0], later[0][:, :, None] * earlier[1] + later[1])


def rounded(float_value):
    return lax.optimization_barrier(float_value.astype(jnp.bfloat16)).astype(jnp.float32)


def fill_slots(rows, sources, places, slot_count):
    picked = rows[sources]
    return jnp.zeros((slot_count, rows.shape[1]), rows.dtype).at[places].set(picked)


def shards(
    skip_path_vectors,
    asker_raw_scores,
    retain_raw_scores,
    memory_write_entries,
    emit_switch_scores,
    retain_minimum_share,
    extra_shrink_rate,
    lane_rescale_factor,
    emit_projection_array,
    specialist_rescale_factor,
    specialist_switch_proj,
    specialist_raise_proj,
    specialist_lower_proj,
    specialist_choice_ids,
    cluster_chance,
    specialist_duo_scores,
):
    token_count_total = skip_path_vectors.shape[0]
    model_width = skip_path_vectors.shape[1]
    head_depth = lane_rescale_factor.shape[0]
    lanes_on_device = extra_shrink_rate.shape[0]
    retain_share = retain_minimum_share + (1.0 - retain_minimum_share) * jax.nn.sigmoid(
        retain_raw_scores.astype(jnp.float32)
    )
    retain_share = retain_share.reshape(token_count_total, lanes_on_device, head_depth)
    shrink_log_rate = jnp.log(retain_share) + extra_shrink_rate.T[:, :, None]
    key_rows = 1.0 - retain_share
    queries = jax.nn.silu(asker_raw_scores.astype(jnp.float32)).reshape(
        token_count_total, lanes_on_device, head_depth
    )
    values = memory_write_entries.astype(jnp.float32).reshape(
        token_count_total, lanes_on_device, head_depth
    )
    cumulative = jnp.cumsum(shrink_log_rate, axis=0)
    query_tilde = queries * jnp.exp(cumulative)
    key_tilde = key_rows * jnp.exp(-cumulative)
    causal = jnp.arange(token_count_total)[:, None] >= jnp.arange(token_count_total)[None, :]
    scores = jnp.einsum("thd,shd->hts", query_tilde, key_tilde, precision=PRECISE)
    scores = jnp.where(causal[None], scores, 0.0)
    inside = jnp.einsum("hts,shv->thv", scores, values, precision=PRECISE)
    totals = jnp.exp(cumulative[-1])
    own_state = jnp.einsum("shd,shv->hdv", key_tilde * totals[None], values, precision=PRECISE)
    identity = (jnp.ones_like(totals), jnp.zeros_like(own_state))
    carried = prefix_by_axis((totals, own_state), SP, chain_join, identity)
    outside = jnp.einsum("thd,hdv->thv", query_tilde, carried[1], precision=PRECISE)
    readout = inside + outside
    normed_heads = readout * lax.rsqrt(jnp.mean(readout * readout, axis=-1, keepdims=True) + EPS)
    gated_out = (
        normed_heads
        * lane_rescale_factor
        * jax.nn.silu(
            emit_switch_scores.astype(jnp.float32).reshape(
                token_count_total, lanes_on_device, head_depth
            )
        )
    )
    mixer_out = gated_out.reshape(token_count_total, lanes_on_device * head_depth).astype(
        jnp.bfloat16
    )
    projected = rounded(
        jnp.dot(mixer_out, emit_projection_array, preferred_element_type=jnp.float32)
    )
    tp_size = lax.axis_size(TP)
    sp_size = lax.axis_size(SP)
    local_experts = specialist_switch_proj.shape[0]
    experts = local_experts * sp_size
    top_count = specialist_choice_ids.shape[1]
    capacity = 3 * token_count_total * top_count // (2 * experts)
    flat_ids = specialist_choice_ids.reshape(-1)
    matches = (flat_ids[:, None] == jnp.arange(experts, dtype=jnp.int32)[None, :]).astype(jnp.int32)
    before = jnp.cumsum(matches, axis=0) - matches
    places = flat_ids * capacity + jnp.sum(before * matches, axis=1)
    sources = jnp.arange(token_count_total * top_count, dtype=jnp.int32) // top_count
    col_width = model_width // tp_size
    col_start = lax.axis_index(TP) * col_width
    own_cols = sent_and_summed(projected.astype(jnp.bfloat16), TP, 1)
    input_cols = lax.dynamic_slice_in_dim(skip_path_vectors, col_start, col_width, 1)
    resid_cols = (input_cols.astype(jnp.float32) + own_cols).astype(jnp.bfloat16)
    wide_rows = resid_cols.astype(jnp.float32)
    squares = over_axes(jnp.sum(wide_rows * wide_rows, axis=1), TP)
    gain_cols = lax.dynamic_slice_in_dim(specialist_rescale_factor, col_start, col_width, 0)
    normed = (wide_rows * lax.rsqrt(squares / model_width + EPS)[:, None] * gain_cols).astype(
        jnp.bfloat16
    )
    slot_rows = fill_slots(normed, sources, places, experts * capacity).reshape(
        experts, capacity, col_width
    )
    arrived = lax.all_to_all(slot_rows, SP, split_axis=0, concat_axis=0, tiled=True)
    arrived = arrived.reshape(sp_size, local_experts, capacity, col_width)
    piece_cols = whole_of(arrived, TP, 3)
    gate_acts = jnp.einsum(
        "secd,edf->secf", piece_cols, specialist_switch_proj, preferred_element_type=jnp.float32
    )
    up_acts = jnp.einsum(
        "secd,edf->secf", piece_cols, specialist_raise_proj, preferred_element_type=jnp.float32
    )
    hidden = (jax.nn.silu(gate_acts) * up_acts).astype(jnp.bfloat16)
    part_out = rounded(
        jnp.einsum(
            "secf,efd->secd", hidden, specialist_lower_proj, preferred_element_type=jnp.float32
        )
    )
    summed = sent_and_summed(part_out.astype(jnp.bfloat16), TP, 3).astype(jnp.bfloat16)
    returned = lax.all_to_all(
        summed.reshape(sp_size * local_experts, capacity, col_width),
        SP,
        split_axis=0,
        concat_axis=0,
        tiled=True,
    )
    picked = returned.reshape(experts * capacity, col_width)[places].reshape(
        token_count_total, top_count, col_width
    )
    spread_logit = specialist_duo_scores[:, 0] - specialist_duo_scores[:, 1]
    weights = cluster_chance[:, None] * jnp.stack(
        [jax.nn.sigmoid(spread_logit), jax.nn.sigmoid(-spread_logit)], axis=1
    )
    mixed_out = resid_cols.astype(jnp.float32) + jnp.sum(
        weights[:, :, None] * picked.astype(jnp.float32), axis=1
    )
    return mixed_out.astype(jnp.bfloat16)


def solution(mesh):
    finer = Mesh(mesh.devices.reshape(16, 2, 4, 4), ("sp_0", "sp_1", "tp_0", "tp_1"))
    in_specs = (
        P(SP, None),
        P(SP, TP),
        P(SP, TP),
        P(SP, TP),
        P(SP, TP),
        P(TP),
        P(TP, SP),
        P(),
        P(TP, None),
        P(),
        P(SP, None, TP),
        P(SP, None, TP),
        P(SP, TP, None),
        P(SP, None),
        P(SP),
        P(SP, None),
    )
    out_specs = P(SP, TP)
    return jax.shard_map(
        shards, mesh=finer, in_specs=in_specs, out_specs=out_specs, check_vma=False
    )
```

profile of v0, /device:TPU:1, one launch (start us, length us, event | category | flops | bytes accessed | tf_op | source)
XLA Modules:
  0.0 281.4 jit_solution(17848426364625329723)
XLA Ops:
  6.5 1.0 copy.36
  7.6 0.7 broadcast_subtract_fusion
  8.2 0.8 add_bitcast_fusion.1
  10.5 1.2 convolution_convert_fusion.2
  11.8 8.3 %all-gather.4 = bf16[2,129,128]{2,1,0:T(8,128)(2,1)S(1)} all-gather(bf16[1,129,128]{2,1,0:T(8,128)(2,1)S(1)} %maximum_bitcast_fusion), channel_id=2, replica_groups=mesh['sp_0'=16,'sp_1'=2,'tp_0'=4,'tp_1'=4] {'sp_1'}, dimensions={0}, use_global_device_ids=true | all-gather | bytes 99072 | tf_op jit(solution)/shard_map/all_gather | solution.py:31
  20.2 26.3 %all-gather.5 = bf16[16,129,128]{2,1,0:T(8,128)(2,1)S(1)} all-gather(bf16[1,129,128]{2,1,0:T(8,128)(2,1)S(1)} %maximum_bitcast_fusion.1), channel_id=3, replica_groups=mesh['sp_0'=16,'sp_1'=2,'tp_0'=4,'tp_1'=4] {'sp_0'}, dimensions={0}, use_global_device_ids=true | all-gather | bytes 561408 | tf_op jit(solution)/shard_map/all_gather | solution.py:31
  46.7 0.5 convolution_select_fusion
  47.2 0.3 convolution_bitcast_fusion.2
  47.5 0.8 multiply_reduce_fusion
  48.5 0.5 convolution_convert_fusion.1
  49.0 1.3 bitcast_bitcast_fusion.1
  50.3 6.9 %all-to-all-start = ((bf16[16,256,128]{2,1,0:T(8,128)(2,1)}), bf16[16,256,128]{2,1,0:T(8,128)(2,1)S(1)}, u32[]{:S(2)}, u32[]{:S(2)}) async-start(bf16[16,256,128]{2,1,0:T(8,128)(2,1)} %bitcast_bitcast_fusion.1), calls=%async_computation | async-start | bytes 2097152 | tf_op jit(solution)/shard_map/all_to_all | solution.py:67
  57.7 1.2 reduce-window.16
  59.4 0.8 dynamic_slice.7
  60.3 9.1 %all-to-all-done = bf16[16,256,128]{2,1,0:T(8,128)(2,1)S(1)} async-done(((bf16[16,256,128]{2,1,0:T(8,128)(2,1)}), bf16[16,256,128]{2,1,0:T(8,128)(2,1)S(1)}, u32[]{:S(2)}, u32[]{:S(2)}) %all-to-all-start) | async-done | bytes 1048608 | tf_op jit(solution)/shard_map/all_to_all | solution.py:67
  69.6 1.0 fusion.24
  70.5 7.0 %psum.14 = f32[256]{0:T(256)S(1)} all-reduce(f32[256]{0:T(256)S(1)} %get-tuple-element.7), channel_id=1, replica_groups=mesh['sp_0'=16,'sp_1'=2,'tp_0'=4,'tp_1'=4] {'tp_0'}, use_global_device_ids=true, to_apply=%region_8.9 | all-reduce | flops 256 | bytes 2048 | tf_op jit(solution)/shard_map/psum | solution.py:72
  77.6 6.6 %psum.15 = f32[256]{0:T(256)S(1)} all-reduce(f32[256]{0:T(256)S(1)} %psum.14), channel_id=1, replica_groups=mesh['sp_0'=16,'sp_1'=2,'tp_0'=4,'tp_1'=4] {'tp_1'}, use_global_device_ids=true, to_apply=%region_9.10 | all-reduce | flops 256 | bytes 2048 | tf_op jit(solution)/shard_map/psum | solution.py:72
  84.2 3.0 %scatter_custom_fusion = bf16[768,128]{1,0:T(8,128)(2,1)S(1)} fusion(s32[512]{0:T(512)S(1)} %bitcast.261, bf16[256,128]{1,0:T(8,128)(2,1)S(1)} %fusion.26, s32[1024]{0:T(1024)S(1)} %pad_clamp_fusion.1, bf16[]{:T(256)} %constant.102.clone.1), kind=kCustom, calls=%fused_computation.52 | custom fusion | bytes 196610 | tf_op jit(solution)/shard_map/scatter | solution.py:92
  87.3 37.7 %all_to_all.20 = bf16[32,24,128]{2,1,0:T(8,128)(2,1)S(1)} all-to-all(bf16[32,24,128]{2,1,0:T(8,128)(2,1)S(1)} %bitcast.259), channel_id=1, replica_groups=mesh['sp_0'=16,'sp_1'=2,'tp_0'=4,'tp_1'=4] {'sp_0','sp_1'}, dimensions={0} | all-to-all | bytes 393216 | tf_op jit(solution)/shard_map/all_to_all | solution.py:183
  125.0 15.6 %all-gather.2 = bf16[32,24,512]{2,1,0:T(8,128)(2,1)} all-gather(bf16[32,24,128]{2,1,0:T(8,128)(2,1)S(1)} %all_to_all.20), channel_id=4, replica_groups=mesh['sp_0'=16,'sp_1'=2,'tp_0'=4,'tp_1'=4] {'tp_1'}, dimensions={2}, use_global_device_ids=true | all-gather | bytes 983040 | tf_op jit(solution)/shard_map/all_gather | solution.py:78
  140.6 37.7 %all-gather.8.cloned.1.call-done = bf16[32,24,2048]{2,1,0:T(8,128)(2,1)} async-done(((bf16[32,24,512]{2,1,0:T(8,128)(2,1)}), bf16[32,24,2048]{2,1,0:T(8,128)(2,1)}) %all-gather.8.cloned.1.call-update) | async-done | bytes 3145744 | tf_op jit(solution)/shard_map/all_gather | solution.py:78
  178.3 3.8 %convolution_bitcast_fusion.1 = f32[32,1,24,256]{3,2,0,1:T(8,128)} fusion(bf16[32,24,2048]{2,1,0:T(8,128)(2,1)} %all-gather.8.cloned.1.call-done, bf16[1,2048,256]{2,1,0:T(8,128)(2,1)S(1)} %copy-done.10), kind=kOutput, calls=%fused_computation.9 | convolution fusion | flops 805306368 | bytes 4980736 | tf_op jit(solution)/shard_map/secd,edf->secf/dot_general | solution.py:186
  182.1 7.2 %fusion = bf16[32,1,24,2048]{3,2,0,1:T(8,128)(2,1)} fusion(bf16[1,256,2048]{2,1,0:T(8,128)(2,1)S(1)} %copy-done, bf16[32,24,2048]{2,1,0:T(8,128)(2,1)} %all-gather.8.cloned.1.call-done, bf16[1,2048,256]{2,1,0:T(8,128)(2,1)S(1)} %copy-done.11, f32[32,1,24,256]{3,2,0,1:T(8,128)} %convolution_bitcast_fusion.1), kind=kOutput, calls=%fused_computation.5 | convolution fusion | flops 1613365248 | bytes 9175040 | tf_op jit(solution)/shard_map/secf,efd->secd/dot_general | solution.py:194
  189.2 2.7 bitcast_bitcast_fusion
  191.9 43.8 %all_to_all.21 = bf16[16,32,1,24,128]{4,3,1,2,0:T(8,128)(2,1)} all-to-all(bf16[16,32,1,24,128]{4,3,1,2,0:T(8,128)(2,1)S(1)} %bitcast_bitcast_fusion), channel_id=1, replica_groups=mesh['sp_0'=16,'sp_1'=2,'tp_0'=4,'tp_1'=4] {'tp_0','tp_1'}, dimensions={0} | all-to-all | bytes 6291456 | tf_op jit(solution)/shard_map/all_to_all | solution.py:67
  235.8 3.1 %reduce_sum.64 = bf16[32,24,128]{2,1,0:T(8,128)(2,1)} reduce(bf16[16,32,1,24,128]{4,3,1,2,0:T(8,128)(2,1)} %all_to_all.21, bf16[]{:T(256)} %constant.102.clone.1), dimensions={0,2}, to_apply=%region_11.12 | reduce | flops 1474560 | bytes 3342338 | tf_op jit(solution)/shard_map/reduce_sum | solution.py:68
  238.8 14.5 %all-to-all-start.3 = ((bf16[32,24,128]{2,1,0:T(8,128)(2,1)}), bf16[32,24,128]{2,1,0:T(8,128)(2,1)S(1)}, u32[]{:S(2)}, u32[]{:S(2)}) async-start(bf16[32,24,128]{2,1,0:T(8,128)(2,1)} %reduce_sum.64), calls=%async_computation.3 | async-start | bytes 393216 | tf_op jit(solution)/shard_map/all_to_all | solution.py:199
  253.6 18.6 %all-to-all-done.3 = bf16[32,24,128]{2,1,0:T(8,128)(2,1)S(1)} async-done(((bf16[32,24,128]{2,1,0:T(8,128)(2,1)}), bf16[32,24,128]{2,1,0:T(8,128)(2,1)S(1)}, u32[]{:S(2)}, u32[]{:S(2)}) %all-to-all-start.3) | async-done | bytes 196640 | tf_op jit(solution)/shard_map/all_to_all | solution.py:199
  272.1 1.3 gather_fusion
  273.5 0.4 fusion.11
  273.9 0.7 fusion.27
  (73 shorter events, 3.4 us)
Async XLA Ops:
  6.5 175.5 %copy-start = (bf16[1,256,2048]{2,1,0:T(8,128)(2,1)S(1)}, bf16[1,256,2048]{2,1,0:T(8,128)(2,1)}, u32[]{:S(2)}) copy-start(bf16[1,256,2048]{2,1,0:T(8,128)(2,1)} %param.28) | copy-start | bytes 3145732
  6.5 40.1 %copy-start.8 = (f32[128]{0:T(128)S(1)}, f32[128]{0:T(128)}, u32[]{:S(2)}) copy-start(f32[128]{0:T(128)} %param.21) | copy-start | bytes 1540
  6.5 40.7 %copy-start.2 = (bf16[256,128]{1,0:T(8,128)(2,1)S(1)}, bf16[256,128]{1,0:T(8,128)(2,1)}, u32[]{:S(2)}) copy-start(bf16[256,128]{1,0:T(8,128)(2,1)} %param.19) | copy-start | bytes 196612
  6.5 40.0 %copy-start.3 = (bf16[256,128]{1,0:T(8,128)(2,1)S(1)}, bf16[256,128]{1,0:T(8,128)(2,1)}, u32[]{:S(2)}) copy-start(bf16[256,128]{1,0:T(8,128)(2,1)} %param.17) | copy-start | bytes 196612
  10.5 37.8 %copy-start.4 = (bf16[256,128]{1,0:T(8,128)(2,1)S(1)}, bf16[256,128]{1,0:T(8,128)(2,1)}, u32[]{:S(2)}) copy-start(bf16[256,128]{1,0:T(8,128)(2,1)} %param.20) | copy-start | bytes 196612
  10.5 37.9 %copy-start.1 = (bf16[128,2048]{1,0:T(8,128)(2,1)S(1)}, bf16[128,2048]{1,0:T(8,128)(2,1)}, u32[]{:S(2)}) copy-start(bf16[128,2048]{1,0:T(8,128)(2,1)} %param.24) | copy-start | bytes 1572868
  10.5 37.9 %copy-start.9 = (f32[128]{0:T(128)S(1)}, f32[128]{0:T(128)}, u32[]{:S(2)}) copy-start(f32[128]{0:T(128)} %param.23) | copy-start | bytes 1540
  48.3 8.9 %copy-start.5 = (s32[256,2]{0,1:T(2,128)S(1)}, s32[256,2]{0,1:T(2,128)}, u32[]{:S(2)}) copy-start(s32[256,2]{0,1:T(2,128)} %param.29) | copy-start | bytes 6148
  50.3 128.0 %copy-start.10 = (bf16[1,2048,256]{2,1,0:T(8,128)(2,1)S(1)}, bf16[1,2048,256]{2,1,0:T(8,128)(2,1)}, u32[]{:S(2)}) copy-start(bf16[1,2048,256]{2,1,0:T(8,128)(2,1)} %param.26) | copy-start | bytes 3145732
  50.3 19.1 %all-to-all-start = ((bf16[16,256,128]{2,1,0:T(8,128)(2,1)}), bf16[16,256,128]{2,1,0:T(8,128)(2,1)S(1)}, u32[]{:S(2)}, u32[]{:S(2)}) async-start(bf16[16,256,128]{2,1,0:T(8,128)(2,1)} %bitcast_bitcast_fusion.1), calls=%async_computation | async-start | bytes 2097152 | tf_op jit(solution)/shard_map/all_to_all | solution.py:67
  57.2 121.1 %all-gather.8.cloned.1.call-start = ((), (), s32[]{:S(2)}) async-start(), calls=%async_computation.4 | async-start | bytes 3932160 | tf_op jit(solution)/shard_map/all_gather | solution.py:78
  140.6 41.5 %copy-start.11 = (bf16[1,2048,256]{2,1,0:T(8,128)(2,1)S(1)}, bf16[1,2048,256]{2,1,0:T(8,128)(2,1)}, u32[]{:S(2)}) copy-start(bf16[1,2048,256]{2,1,0:T(8,128)(2,1)} %param.27) | copy-start | bytes 3145732
  235.8 17.6 %copy-start.6 = (f32[256,2]{0,1:T(2,128)S(1)}, f32[256,2]{0,1:T(2,128)}, u32[]{:S(2)}) copy-start(f32[256,2]{0,1:T(2,128)} %param.31) | copy-start | bytes 6148
  235.8 17.6 %copy-start.7 = (f32[256]{0:T(256)S(1)}, f32[256]{0:T(256)}, u32[]{:S(2)}) copy-start(f32[256]{0:T(256)} %param.30) | copy-start | bytes 3076
  238.8 33.3 %all-to-all-start.3 = ((bf16[32,24,128]{2,1,0:T(8,128)(2,1)}), bf16[32,24,128]{2,1,0:T(8,128)(2,1)S(1)}, u32[]{:S(2)}, u32[]{:S(2)}) async-start(bf16[32,24,128]{2,1,0:T(8,128)(2,1)} %reduce_sum.64), calls=%async_computation.3 | async-start | bytes 393216 | tf_op jit(solution)/shard_map/all_to_all | solution.py:199
Sparse Core Ops, SparseCore 0:
  140.7 37.4 all-gather.7
where the time goes:
time: 282 us; the launch traced here: 281 us
  blocking collectives  145 us (51%)
  waiting for transfers between devices  65.4 us (23%)
  starting transfers between devices  21.4 us (8%)
  matrix products  14.3 us (5%)
  between operations  13.8 us (5%)
  local copies, waits for them, and re-layouts  12.5 us (4%)
  other arithmetic  8.68 us (3%)
    all_to_all x1, blocking collectives, sent_and_summed(): parts = lax.all_to_all(cut_along(array, dim, count), axis, 0, 0, tiled=True)  43.8 us
    all_to_all x1, blocking collectives, shards(): lax.all_to_all(slot_rows, SP, split_axis=0, concat_axis=0, tiled=True)  37.7 us
    all_gather x1, waiting for transfers between devices, whole_of(): nearer = lax.all_gather(array, axes[-1], axis=dim, tiled=True)  37.7 us
    all_gather x2, blocking collectives, gathered_once(): both, at, found = (lax.all_gather(jnp.concatenate(lines), axis), 0, {})  34.6 us
    all_to_all x1, waiting for transfers between devices, shards(): lax.all_to_all(summed.reshape(sp_size * local_experts, capacity, col_widt...  18.6 us
    all_gather x1, blocking collectives, whole_of(): nearer = lax.all_gather(array, axes[-1], axis=dim, tiled=True)  15.6 us
    all_to_all x1, starting transfers between devices, shards(): lax.all_to_all(summed.reshape(sp_size * local_experts, capacity, col_widt...  14.5 us
    psum x2, blocking collectives, over_axes(): return functools.reduce(lax.psum, axes, array)  13.6 us
  transfers between devices with their start and end apart: 3, of which 3 were waited for; matrix products, arithmetic and copies ran while one was open for 1% of the time, Pallas kernels for 0%

commit v1 on v0

v1 whole, which is shorter than its diff:
```python
import functools

import jax
import jax.numpy as jnp
from jax import lax
from jax.experimental import pallas as pl
from jax.experimental.pallas import tpu as pltpu
from jax.sharding import Mesh
from jax.sharding import PartitionSpec as P

AXES = ("z", "c", "y", "x")
SP = ("z", "c")
TP = ("y", "x")
EPS = 1e-06
BF = jnp.bfloat16
F32 = jnp.float32
HIGH = lax.Precision.HIGHEST
MESH = pl.DeviceIdType.MESH
CHUNK = 4
TILE = 8


def dims_of(a, b, left, right, precision=None):
    return lax.dot_general(
        a, b, (((left,), (right,)), ((), ())), precision=precision, preferred_element_type=F32
    )


def z_steps(count):
    steps = [0]
    for far in range(1, count // 2 + 1):
        steps += [far, -far]
    return steps[:count]


def column_of(row, eye):
    return jnp.sum(jnp.where(eye, row, 0.0), axis=1, keepdims=True)


class Wire:
    def __init__(self, sends, recvs):
        self.sends, self.recvs, self.used, self.started = sends, recvs, 0, []

    def slots(self, count):
        first = self.used
        self.used += count
        return first

    def copy(self, src, dst, number, device):
        return pltpu.make_async_remote_copy(
            src_ref=src,
            dst_ref=dst,
            send_sem=self.sends.at[number],
            recv_sem=self.recvs.at[number],
            device_id=device,
            device_id_type=MESH,
        )

    def send(self, src, dst, number, device):
        copy = self.copy(src, dst, number, device)
        copy.start()
        self.started.append(copy)

    def arrived(self, dst, number, device):
        self.copy(dst, dst, number, device).wait_recv()


def semaphore_count(nz, nc, tp):
    blocks = nz * nc
    chunks = max(1, nz // CHUNK)
    return 1 + 3 + 3 + 1 + 2 * blocks + (chunks * 32 + 16 if tp > 1 else 0)


def kernel(
    sizes,
    asker,
    retain,
    entries,
    emit,
    least,
    extra,
    lane_gain,
    row_gain,
    ids,
    chance,
    duo,
    skip_hbm,
    project_hbm,
    switch_hbm,
    raise_hbm,
    lower_hbm,
    out,
    skip,
    project,
    switch,
    raised,
    lower,
    state_own,
    state_first,
    half_out,
    half_in,
    near,
    far,
    back_out,
    back_in,
    prefix,
    query_hat,
    inside,
    gates,
    select_in,
    select_out,
    route,
    mix_part,
    mix_one,
    mix_two,
    mix_sum,
    mix_three,
    mix_four,
    slots,
    rows,
    normed,
    part,
    red_one,
    red_two,
    red_sum,
    red_three,
    red_four,
    finished,
    returned,
    local_sems,
    sends,
    recvs,
):
    nz, nc, ny, nx, tokens, cap = sizes
    tp = ny * nx
    groups = nz // 4
    half = tokens // 2
    z, c, y, x = (lax.axis_index(a) for a in AXES)
    me_sp = z * nc + c
    wire = Wire(sends, recvs)
    steps = z_steps(nz)
    chunks = nz // CHUNK

    def device(dz=0, dc=0, dy=0, dx=0):
        return (
            lax.rem(z + (dz + nz), nz),
            lax.rem(c + dc, nc),
            lax.rem(y + (dy + ny), ny),
            lax.rem(x + (dx + nx), nx),
        )

    partner = device(dc=1)
    barrier = pltpu.get_barrier_semaphore()
    peers = [device(dz=dz, dc=dc) for dz in steps for dc in range(nc) if (dz, dc) != (0, 0)]
    if tp > 1:
        peers += [device(dy=1), device(dy=-1), device(dx=1), device(dx=-1)]
    for peer in peers:
        pl.semaphore_signal(barrier, inc=1, device_id=peer, device_id_type=MESH)

    my_cols = pl.ds(pl.multiple_of((y * nx + x) * 128, 128), 128)
    loads = [
        pltpu.make_async_copy(src, dst, local_sems.at[i])
        for i, (src, dst) in enumerate(
            [
                (project_hbm, project),
                (skip_hbm.at[:, my_cols], skip),
                (switch_hbm, switch),
                (raise_hbm, raised),
                (lower_hbm, lower),
            ]
        )
    ]
    for load in loads:
        load.start()

    spots = lax.broadcasted_iota(jnp.int32, (half, half), 0)
    other = lax.broadcasted_iota(jnp.int32, (half, half), 1)
    causal = spots >= other
    causal_ones = jnp.where(causal, 1.0, 0.0).astype(F32)
    eye_half = spots == other

    def decays(b):
        mine = pl.ds(b * half, half)
        floor = least[...]
        share = floor + (1.0 - floor) * jax.nn.sigmoid(retain[mine, :].astype(F32))
        logs = jnp.log(share) + column_of(extra[:, b * half : (b + 1) * half], eye_half)
        total = jnp.dot(causal_ones, logs, precision=HIGH, preferred_element_type=F32)
        return total, 1.0 - share

    states, lasts, kept = [], [], []
    for b in range(2):
        total, keys = decays(b)
        last = total[half - 1 : half, :]
        ending = keys * jnp.exp(last - total)
        values = entries[b * half : (b + 1) * half, :].astype(F32)
        states.append(dims_of(values, ending, 0, 0, HIGH))
        lasts.append(last)
        kept.append((total, keys))
    own_decay = jnp.exp(lasts[0] + lasts[1])
    state_first[...] = states[0]
    state_own[...] = jnp.exp(lasts[1]) * states[0] + states[1]

    tail_row = lax.broadcasted_iota(jnp.int32, (16, 128), 0)

    def pack(ref, value, decay):
        top = decay.astype(BF)
        low = (decay - top.astype(F32)).astype(BF)
        ref[0:64, :] = value.astype(BF)
        tail = jnp.where(
            tail_row == 0, top.astype(F32), jnp.where(tail_row == 1, low.astype(F32), 0.0)
        )
        ref[64:80, :] = tail.astype(BF)

    def unpack(ref):
        tail = ref[64:80, :].astype(F32)
        return ref[0:64, :].astype(F32), tail[0:1, :] + tail[1:2, :]

    first_core = c == 0
    mine_half = jnp.where(first_core, state_own[0:64, :], state_own[64:128, :])
    theirs_half = jnp.where(first_core, state_own[64:128, :], state_own[0:64, :])
    pack(half_out, theirs_half, own_decay)

    pl.semaphore_wait(barrier, len(peers))

    n_half = wire.slots(1)
    n_near = wire.slots(3)
    n_far = wire.slots(3)
    n_back = wire.slots(1)
    wire.send(half_out, half_in, n_half, partner)

    def score_block(b):
        total, keys = kept[b]
        mine = pl.ds(b * half, half)
        middle = total[half // 2 - 1 : half // 2, :]
        asked = jax.nn.silu(asker[mine, :].astype(F32))
        query_hat[mine, :] = asked * jnp.exp(total)
        scores = dims_of(
            asked * jnp.exp(total - middle), keys * jnp.exp(middle - total), 1, 1, HIGH
        )
        scores = jnp.where(causal, scores, 0.0)
        values = entries[mine, :].astype(F32)
        inside[mine, :] = jnp.dot(scores, values, precision=HIGH, preferred_element_type=F32)
        gates[mine, :] = lane_gain[...] * jax.nn.silu(emit[mine, :].astype(F32))

    wire.arrived(half_in, n_half, partner)
    theirs, their_decay = unpack(half_in)
    s0 = jnp.where(first_core, mine_half, theirs)
    s1 = jnp.where(first_core, theirs, mine_half)
    d0 = jnp.where(first_core, own_decay, their_decay)
    d1 = jnp.where(first_core, their_decay, own_decay)
    group, place = z // 4, lax.rem(z, 4)
    pack(near.at[place], d1 * s0 + s1, d0 * d1)

    def in_group(j):
        return (group * 4 + lax.rem(place + j, 4), c, y, x)

    for j in (1, 2, 3):
        wire.send(near.at[place], near.at[place], n_near + j - 1, in_group(j))

    score_block(0)
    score_block(1)

    for j in (1, 2, 3):
        sender = lax.rem(place + 4 - j, 4)
        wire.arrived(near.at[sender], n_near + j - 1, in_group(4 - j))
    before = jnp.zeros((64, 128), F32)
    before_decay = jnp.ones((1, 128), F32)
    total_state, total_decay = before, before_decay
    for j in range(4):
        value, decay = unpack(near.at[j])
        total_state = decay * total_state + value
        total_decay = decay * total_decay
        earlier = j < place
        before = jnp.where(earlier, decay * before + value, before)
        before_decay = jnp.where(earlier, decay * before_decay, before_decay)
    pack(far.at[group], total_state, total_decay)

    def to_group(j):
        return (lax.rem(z + 4 * j, nz), c, y, x)

    for j in range(1, groups):

        @pl.when(group + j < groups)
        def _():
            wire.copy(far.at[group], far.at[group], n_far + j - 1, to_group(j)).start()

    tok_row = lax.broadcasted_iota(jnp.int32, (tokens, tokens), 0)
    tok_col = lax.broadcasted_iota(jnp.int32, (tokens, tokens), 1)
    eye = tok_row == tok_col
    earlier_ones = jnp.where(tok_row < tok_col, 1.0, 0.0).astype(BF)
    experts = nz * nc
    expert_at = lax.broadcasted_iota(jnp.int32, (experts, tokens), 0)
    named = [jnp.where(expert_at == ids[j : j + 1, :], 1.0, 0.0).astype(F32) for j in range(2)]
    counts = jnp.dot(
        (named[0] + named[1]).astype(BF), earlier_ones, preferred_element_type=F32
    )
    slot_rows = [
        ids[j : j + 1, :].astype(F32) * cap + jnp.sum(counts * named[j], axis=0, keepdims=True)
        for j in range(2)
    ]
    slot_at = lax.broadcasted_iota(jnp.int32, (experts * cap, tokens), 0).astype(F32)
    select_in[...] = jnp.where(
        slot_at == slot_rows[0], 1.0, jnp.where(slot_at == slot_rows[1], 1.0, 0.0)
    ).astype(BF)
    slot_along = lax.broadcasted_iota(jnp.int32, (tokens, experts * cap), 1).astype(F32)
    spread = duo[0:1, :] - duo[1:2, :]
    for j in range(2):
        select_out[j] = jnp.where(
            slot_along == column_of(slot_rows[j], eye), 1.0, 0.0
        ).astype(BF)
        weight = chance[...] * jax.nn.sigmoid(spread if j == 0 else -spread)
        route[j] = jnp.broadcast_to(column_of(weight, eye), (tokens, 128))

    prefix[...] = jnp.zeros((64, 128), F32)
    for j in range(groups - 1):

        @pl.when(j < group)
        def _():
            sender = j
            number = n_far + group - 1 - j
            wire.arrived(far.at[sender], number, to_group(0))
            value, decay = unpack(far.at[sender])
            prefix[...] = decay * prefix[...] + value

    start = before_decay * prefix[...] + before
    after_first = d0 * start + s0
    back_out[...] = jnp.where(first_core, after_first, start).astype(BF)
    wire.send(back_out, back_in, n_back, partner)
    own_start = jnp.where(first_core, start, after_first)
    wire.arrived(back_in, n_back, partner)
    got = back_in[...].astype(F32)
    carried = jnp.concatenate(
        [jnp.where(first_core, own_start, got), jnp.where(first_core, got, own_start)], axis=0
    )
    for j in range(1, groups):

        @pl.when(group + j < groups)
        def _():
            wire.copy(far.at[group], far.at[group], n_far + j - 1, to_group(j)).wait_send()

    second = jnp.exp(lasts[0]) * carried + state_first[...]
    loads[0].wait()
    for b, state in enumerate((carried, second)):
        mine = pl.ds(b * half, half)
        readout = inside[mine, :] + dims_of(query_hat[mine, :], state, 1, 1, HIGH)
        mean = jnp.mean(readout * readout, axis=1, keepdims=True)
        mixed = (readout * lax.rsqrt(mean + EPS) * gates[mine, :]).astype(BF)
        for t in range(0, tp, 2):
            wide = jnp.dot(
                mixed, project[:, t * 128 : (t + 2) * 128], preferred_element_type=F32
            )
            for u in range(t, min(t + 2, tp)):
                mix_part[u // nx, u % nx, b] = (
                    wide[:, (u - t) * 128 : (u - t + 1) * 128]
                    .reshape(2, half // 2, 128)
                    .astype(BF)
                )

    class Reduce:
        def __init__(self, source, lo, n, one, two, total, three, four):
            self.source, self.lo, self.n = source, lo, n
            self.bufs = (one, two, total, three, four)
            self.first = wire.slots(16)

        def at(self, k, f, g):
            rest = (k, pl.ds(self.lo, self.n))
            return self.source.at[(f, g) + rest] if k == 0 else self.source.at[(g, f) + rest]

        def axes(self, k):
            f, g = (y, x) if k == 0 else (x, y)
            name_f, name_g = ("dy", "dx") if k == 0 else ("dx", "dy")
            return f, g, (lambda d: device(**{name_f: d})), (lambda d: device(**{name_g: d}))

        def number(self, k, step, way):
            return self.first + k * 8 + step * 2 + way

        def step_one(self):
            one = self.bufs[0]
            for k in range(2):
                f, g, to_f, to_g = self.axes(k)
                across = lax.rem(f + 2, 4)
                for way, delta in ((0, 1), (1, -1)):
                    wire.send(
                        self.at(k, across, pl.ds(2 * way, 2)),
                        one.at[k, way],
                        self.number(k, 0, way),
                        to_f(delta),
                    )

        def step_two(self):
            one, two = self.bufs[0], self.bufs[1]
            for k in range(2):
                f, g, to_f, to_g = self.axes(k)
                for way, delta in ((0, 1), (1, -1)):
                    wire.arrived(one.at[k, way], self.number(k, 0, way), to_f(-delta))
                    mine = self.at(k, lax.rem(f + delta + 4, 4), pl.ds(2 * way, 2))
                    mine[...] = (mine[...].astype(F32) + one[k, way].astype(F32)).astype(BF)
            for k in range(2):
                f, g, to_f, to_g = self.axes(k)
                for way, delta in ((0, 1), (1, -1)):
                    wire.send(
                        self.at(k, lax.rem(f + delta + 4, 4), pl.ds(0, 4)),
                        two.at[k, way],
                        self.number(k, 1, way),
                        to_f(delta),
                    )

        def step_three(self):
            two, total, three = self.bufs[1], self.bufs[2], self.bufs[3]
            h = self.n // 2
            for k in range(2):
                f, g, to_f, to_g = self.axes(k)
                for way, delta in ((0, 1), (1, -1)):
                    wire.arrived(two.at[k, way], self.number(k, 1, way), to_f(-delta))
                total[k] = (
                    self.at(k, f, pl.ds(0, 4))[...].astype(F32)
                    + two[k, 0].astype(F32)
                    + two[k, 1].astype(F32)
                ).astype(BF)
            for k in range(2):
                f, g, to_f, to_g = self.axes(k)
                for way, delta in ((0, 1), (1, -1)):
                    wire.send(
                        total.at[k, lax.rem(g + 2, 4), pl.ds(way * h, h)],
                        three.at[k, way],
                        self.number(k, 2, way),
                        to_g(delta),
                    )

        def step_four(self):
            total, three, four = self.bufs[2], self.bufs[3], self.bufs[4]
            h = self.n // 2
            for k in range(2):
                f, g, to_f, to_g = self.axes(k)
                for way, delta in ((0, 1), (1, -1)):
                    wire.arrived(three.at[k, way], self.number(k, 2, way), to_g(-delta))
                    mine = total.at[k, lax.rem(g + delta + 4, 4), pl.ds(way * h, h)]
                    mine[...] = (mine[...].astype(F32) + three[k, way].astype(F32)).astype(BF)
            for k in range(2):
                f, g, to_f, to_g = self.axes(k)
                for way, delta in ((0, 1), (1, -1)):
                    wire.send(
                        total.at[k, lax.rem(g + delta + 4, 4)],
                        four.at[k, way],
                        self.number(k, 3, way),
                        to_g(delta),
                    )

        def result(self, k):
            two, four = self.bufs[1], self.bufs[4]
            f, g, to_f, to_g = self.axes(k)
            for way, delta in ((0, 1), (1, -1)):
                wire.arrived(four.at[k, way], self.number(k, 3, way), to_g(-delta))
            return (
                self.at(k, f, g)[...].astype(F32)
                + two[k, 0, g].astype(F32)
                + two[k, 1, g].astype(F32)
                + four[k, 0].astype(F32)
                + four[k, 1].astype(F32)
            )

    loads[1].wait()
    if tp > 1:
        mix = Reduce(mix_part, 0, 2, mix_one, mix_two, mix_sum, mix_three, mix_four)
        mix.step_one()
        mix.step_two()
        mix.step_three()
        mix.step_four()
        own_cols = [mix.result(k).reshape(half, 128) for k in range(2)]
    else:
        own_cols = [mix_part[0, 0, k].astype(F32).reshape(half, 128) for k in range(2)]
    for k in range(2):
        mine = pl.ds(k * half, half)
        skip[mine, :] = (skip[mine, :].astype(F32) + own_cols[k]).astype(BF)

    tiles = cap // TILE
    slots[...] = (
        jnp.dot(select_in[...], skip[...], preferred_element_type=F32)
        .reshape(experts, tiles, TILE, 128)
        .astype(BF)
    )
    rows[y, x, 0, 0] = slots[me_sp]
    n_out = wire.slots(nz * nc)
    for i, dz in enumerate(steps):
        for dc in range(nc):
            if (dz, dc) == (0, 0):
                continue
            there = device(dz=dz, dc=dc)
            wire.send(
                slots.at[there[0] * nc + there[1]],
                rows.at[y, x, dc, i],
                n_out + i * nc + dc,
                there,
            )

    class Chunk:
        def __init__(self, number):
            self.lo = number * CHUNK
            self.number = number
            if tp > 1:
                self.first = wire.slots(16)
                self.red = Reduce(
                    part,
                    self.lo,
                    CHUNK,
                    *(b.at[number] for b in (red_one, red_two, red_sum, red_three, red_four)),
                )

        def at(self, k, p, s, lo=0, n=CHUNK):
            rest = (k, pl.ds(self.lo + lo, n))
            return rows.at[(s, p) + rest] if k == 0 else rows.at[(p, s) + rest]

        def axes(self, k):
            p, s = (x, y) if k == 0 else (y, x)
            name_p, name_s = ("dx", "dy") if k == 0 else ("dy", "dx")
            return p, s, (lambda d: device(**{name_p: d})), (lambda d: device(**{name_s: d}))

        def sem(self, k, step, way):
            return self.first + k * 8 + step * 2 + way

        def gather_one(self):
            for i in range(self.lo, self.lo + CHUNK):
                for dc in range(nc):
                    if (steps[i], dc) != (0, 0):
                        wire.arrived(
                            rows.at[y, x, dc, i], n_out + i * nc + dc, device(dz=-steps[i], dc=dc)
                        )
            if tp == 1:
                return
            for k in range(2):
                p, s, to_p, to_s = self.axes(k)
                for way, delta in ((0, 1), (1, -1)):
                    mine = self.at(k, p, s)
                    wire.send(mine, mine, self.sem(k, 0, way), to_p(delta))

        def gather_two(self):
            h = CHUNK // 2
            for k in range(2 if tp > 1 else 0):
                p, s, to_p, to_s = self.axes(k)
                for way, delta in ((0, 1), (1, -1)):
                    came = lax.rem(p - delta + 4, 4)
                    wire.arrived(self.at(k, came, s), self.sem(k, 0, way), to_p(-delta))
                    onward = self.at(k, came, s, way * h, h)
                    wire.send(onward, onward, self.sem(k, 1, way), to_p(delta))

        def gather_three(self):
            h = CHUNK // 2
            for k in range(2 if tp > 1 else 0):
                p, s, to_p, to_s = self.axes(k)
                across = lax.rem(p + 2, 4)
                for way, delta in ((0, 1), (1, -1)):
                    wire.arrived(
                        self.at(k, across, s, way * h, h), self.sem(k, 1, way), to_p(-delta)
                    )
                mine = self.at(k, pl.ds(0, 4), s)
                for way, delta in ((0, 1), (1, -1)):
                    wire.send(mine, mine, self.sem(k, 2, way), to_s(delta))

        def gather_four(self):
            for k in range(2 if tp > 1 else 0):
                p, s, to_p, to_s = self.axes(k)
                for way, delta in ((0, 1), (1, -1)):
                    came = lax.rem(s - delta + 4, 4)
                    wire.arrived(
                        self.at(k, pl.ds(0, 4), came), self.sem(k, 2, way), to_s(-delta)
                    )
                    onward = self.at(k, pl.ds(2 * way, 2), came)
                    wire.send(onward, onward, self.sem(k, 3, way), to_s(delta))

        def experts(self):
            for k in range(2 if tp > 1 else 0):
                p, s, to_p, to_s = self.axes(k)
                across = lax.rem(s + 2, 4)
                for way, delta in ((0, 1), (1, -1)):
                    wire.arrived(
                        self.at(k, pl.ds(2 * way, 2), across), self.sem(k, 3, way), to_s(-delta)
                    )
            span = pl.ds(self.lo, CHUNK)
            count = nc * CHUNK * cap
            squares = jnp.zeros((count, 128), F32)
            for t in range(tp):
                wide = rows[t // nx, t % nx, :, span].astype(F32).reshape(count, 128)
                squares = squares + wide * wide
            scale = lax.rsqrt(jnp.sum(squares, axis=1, keepdims=True) / (tp * 128) + EPS)
            for t in range(tp):
                wide = rows[t // nx, t % nx, :, span].astype(F32).reshape(count, 128)
                cols = slice(t * 128, (t + 1) * 128)
                normed[:, cols] = (wide * scale * row_gain[:, cols]).astype(BF)
            gate_acts = jnp.dot(normed[...], switch[...], preferred_element_type=F32)
            up_acts = jnp.dot(normed[...], raised[...], preferred_element_type=F32)
            hidden = (jax.nn.silu(gate_acts) * up_acts).astype(BF)
            for t in range(0, tp, 2):
                wide = jnp.dot(
                    hidden, lower[:, t * 128 : (t + 2) * 128], preferred_element_type=F32
                )
                for u in range(t, min(t + 2, tp)):
                    part[u // nx, u % nx, :, span] = (
                        wide[:, (u - t) * 128 : (u - t + 1) * 128]
                        .reshape(nc, CHUNK, tiles, TILE, 128)
                        .astype(BF)
                    )
            if tp > 1:
                self.red.step_one()

        def sum_two(self):
            if tp > 1:
                self.red.step_two()

        def sum_three(self):
            if tp > 1:
                self.red.step_three()

        def sum_four(self):
            if tp > 1:
                self.red.step_four()

        def give_back(self):
            for k in range(2):
                if tp > 1:
                    done = self.red.result(k).astype(BF)
                else:
                    done = part[0, 0, k, pl.ds(self.lo, CHUNK)]
                finished[k, pl.ds(self.lo, CHUNK)] = done
            for i in range(self.lo, self.lo + CHUNK):
                for dc in range(nc):
                    if (steps[i], dc) == (0, 0):
                        returned[me_sp] = finished[0, 0]
                        continue
                    wire.send(
                        finished.at[dc, i],
                        returned.at[me_sp],
                        n_back_rows + i * nc + dc,
                        device(dz=-steps[i], dc=dc),
                    )

    n_back_rows = wire.slots(nz * nc)
    work = [Chunk(n) for n in range(chunks)]
    for load in loads[2:]:
        load.wait()
    order = (
        "gather_one",
        "gather_two",
        "gather_three",
        "gather_four",
        "experts",
        "sum_two",
        "sum_three",
        "sum_four",
        "give_back",
    )
    tasks = sorted((j + 2 * n, n, j) for n in range(chunks) for j in range(len(order)))
    for _, n, j in tasks:
        getattr(work[n], order[j])()

    for i, dz in enumerate(steps):
        for dc in range(nc):
            if (dz, dc) == (0, 0):
                continue
            there = device(dz=dz, dc=dc)
            wire.arrived(
                returned.at[there[0] * nc + there[1]], n_back_rows + i * nc + dc, there
            )
    got_rows = returned[...].astype(F32).reshape(experts * cap, 128).astype(BF)
    result = skip[...].astype(F32)
    for j in range(2):
        picked = jnp.dot(select_out[j], got_rows, preferred_element_type=F32)
        result = result + route[j] * picked
    out[...] = result.astype(BF)
    for copy in wire.started:
        copy.wait_send()


def layer(
    sizes,
    skip_path_vectors,
    asker_raw_scores,
    retain_raw_scores,
    memory_write_entries,
    emit_switch_scores,
    retain_minimum_share,
    extra_shrink_rate,
    lane_rescale_factor,
    emit_projection_array,
    specialist_rescale_factor,
    specialist_switch_proj,
    specialist_raise_proj,
    specialist_lower_proj,
    specialist_choice_ids,
    cluster_chance,
    specialist_duo_scores,
):
    nz, nc, ny, nx, tokens, cap = sizes
    tp = ny * nx
    width = tp * 128
    hidden = specialist_switch_proj.shape[2]
    half, experts, chunks, tiles = tokens // 2, nz * nc, nz // CHUNK, cap // TILE
    block = (tiles, TILE, 128)
    vmem, anywhere = (
        pl.BlockSpec(memory_space=pltpu.VMEM),
        pl.BlockSpec(memory_space=pl.ANY),
    )
    count = semaphore_count(nz, nc, tp)
    scratch = [
        pltpu.VMEM((tokens, 128), BF),
        pltpu.VMEM((128, width), BF),
        pltpu.VMEM((width, hidden), BF),
        pltpu.VMEM((width, hidden), BF),
        pltpu.VMEM((hidden, width), BF),
        pltpu.VMEM((128, 128), F32),
        pltpu.VMEM((128, 128), F32),
        pltpu.VMEM((80, 128), BF),
        pltpu.VMEM((80, 128), BF),
        pltpu.VMEM((4, 80, 128), BF),
        pltpu.VMEM((nz // 4, 80, 128), BF),
        pltpu.VMEM((64, 128), BF),
        pltpu.VMEM((64, 128), BF),
        pltpu.VMEM((64, 128), F32),
        pltpu.VMEM((tokens, 128), F32),
        pltpu.VMEM((tokens, 128), F32),
        pltpu.VMEM((tokens, 128), F32),
        pltpu.VMEM((experts * cap, tokens), BF),
        pltpu.VMEM((2, tokens, experts * cap), BF),
        pltpu.VMEM((2, tokens, 128), F32),
        pltpu.VMEM((ny, nx, 2, 2, half // 2, 128), BF),
        pltpu.VMEM((2, 2, 2, 2, half // 2, 128), BF),
        pltpu.VMEM((2, 2, 4, 2, half // 2, 128), BF),
        pltpu.VMEM((2, 4, 2, half // 2, 128), BF),
        pltpu.VMEM((2, 2, 1, half // 2, 128), BF),
        pltpu.VMEM((2, 2, 2, half // 2, 128), BF),
        pltpu.VMEM((experts, *block), BF),
        pltpu.VMEM((ny, nx, nc, nz, *block), BF),
        pltpu.VMEM((nc * CHUNK * cap, width), BF),
        pltpu.VMEM((ny, nx, nc, nz, *block), BF),
        pltpu.VMEM((chunks, 2, 2, 2, CHUNK, *block), BF),
        pltpu.VMEM((chunks, 2, 2, 4, CHUNK, *block), BF),
        pltpu.VMEM((chunks, 2, 4, CHUNK, *block), BF),
        pltpu.VMEM((chunks, 2, 2, CHUNK // 2, *block), BF),
        pltpu.VMEM((chunks, 2, 2, CHUNK, *block), BF),
        pltpu.VMEM((nc, nz, *block), BF),
        pltpu.VMEM((experts, *block), BF),
        pltpu.SemaphoreType.DMA((5,)),
        pltpu.SemaphoreType.DMA((count,)),
        pltpu.SemaphoreType.DMA((count,)),
    ]
    return pl.pallas_call(
        functools.partial(kernel, sizes),
        out_shape=jax.ShapeDtypeStruct((tokens, 128), BF),
        in_specs=[vmem] * 11 + [anywhere] * 5,
        out_specs=vmem,
        scratch_shapes=scratch,
        compiler_params=pltpu.CompilerParams(collective_id=0, has_side_effects=True),
    )(
        asker_raw_scores,
        retain_raw_scores,
        memory_write_entries,
        emit_switch_scores,
        retain_minimum_share.reshape(1, 128),
        extra_shrink_rate,
        lane_rescale_factor.reshape(1, 128),
        specialist_rescale_factor.reshape(1, width),
        specialist_choice_ids.T,
        cluster_chance.reshape(1, tokens),
        specialist_duo_scores.T,
        skip_path_vectors,
        emit_projection_array,
        specialist_switch_proj[0],
        specialist_raise_proj[0],
        specialist_lower_proj[0],
    )


def solution(mesh, shape=(16, 2, 4, 4), tokens=256, cap=24):
    finer = Mesh(mesh.devices.reshape(shape), AXES)
    in_specs = (
        P(SP, None),
        P(SP, TP),
        P(SP, TP),
        P(SP, TP),
        P(SP, TP),
        P(TP),
        P(TP, SP),
        P(),
        P(TP, None),
        P(),
        P(SP, None, TP),
        P(SP, None, TP),
        P(SP, TP, None),
        P(SP, None),
        P(SP),
        P(SP, None),
    )
    return jax.shard_map(
        functools.partial(layer, (*shape, tokens, cap)),
        mesh=finer,
        in_specs=in_specs,
        out_specs=P(SP, TP),
        check_vma=False,
    )
```

time: 282 us -> 132 us (0.47)
  blocking collectives: 145 us -> 0 us
  Pallas kernels: 0 us -> 131 us
  waiting for transfers between devices: 65.4 us -> 0 us
  starting transfers between devices: 21.4 us -> 0 us
  matrix products: 14.3 us -> 0 us
  between operations: 13.8 us -> 0.01 us
  local copies, waits for them, and re-layouts: 12.5 us -> 1.47 us
  other arithmetic: 8.68 us -> 0 us
    pallas_call x0 -> x1, Pallas kernels: none -> 131 us  [layer(): pl.pallas_call(functools.partial(kernel, sizes), out_shape=jax.ShapeDtype...]
    all_to_all x2 -> x0, blocking collectives: 81.5 us -> none  [the longest x1 43.8 us: sent_and_summed(): parts = lax.all_to_all(cut_along(array, dim, count), axis, 0, 0, tiled=True)]
    all_gather x3 -> x0, blocking collectives: 50.2 us -> none  [the longest x2 34.6 us: gathered_once(): both, at, found = (lax.all_gather(jnp.concatenate(lines), axis), 0, {})]
    all_gather x1 -> x0, waiting for transfers between devices: 37.7 us -> none  [whole_of(): nearer = lax.all_gather(array, axes[-1], axis=dim, tiled=True)]
    all_to_all x2 -> x0, waiting for transfers between devices: 27.7 us -> none  [the longest x1 18.6 us: shards(): lax.all_to_all(summed.reshape(sp_size * local_experts, capacity, col_widt...]
    all_to_all x2 -> x0, starting transfers between devices: 21.4 us -> none  [the longest x1 14.5 us: shards(): lax.all_to_all(summed.reshape(sp_size * local_experts, capacity, col_widt...]
    dot_general x7 -> x0, matrix products: 14.3 us -> none  [the longest x1 7.17 us: shards(): jnp.einsum('secf,efd->secd', hidden, specialist_lower_proj, preferred_ele...]
    psum x2 -> x0, blocking collectives: 13.6 us -> none  [over_axes(): return functools.reduce(lax.psum, axes, array)]
  transfers between devices with their start and end apart: 3 -> 0, of which waited for: 3 -> 0; matrix products, arithmetic and copies ran while one was open for 1% -> 0% of each run, Pallas kernels for 0% -> 0%
where the time goes in v1:
time: 132 us
  Pallas kernels  131 us (99%)
  local copies, waits for them, and re-layouts  1.47 us (1%)
    pallas_call x1, Pallas kernels, layer(): pl.pallas_call(functools.partial(kernel, sizes), out_shape=jax.ShapeDtype...  131 us

profile of v1, /device:TPU:1, one launch (start us, length us, event | category | flops | bytes accessed | tf_op | source)
XLA Modules:
  0.0 132.1 jit_solution(18278359728120639111)
XLA Ops:
  0.0 130.6 %shard_map.154 = bf16[256,128]{1,0:T(8,128)(2,1)} custom-call(bf16[256,128]{1,0:T(8,128)(2,1)} %asker.1, bf16[256,128]{1,0:T(8,128)(2,1)} %retain.1, bf16[256,128]{1,0:T(8,128)(2,1)} %entries.1, bf16[256,128]{1,0:T(8,128)(2,1)} %emit.1, f32[1,128]{1,0:T(1,128)} %bitcast.16, f32[1,256]{1,0:T(1,128)} %extra.1, f32[1,128]{1,0:T(1,128)} %bitcast.17, ...), custom_call_target="tpu_custom_call" | custom-call | tf_op jit(solution)/shard_map/pallas_call | solution.py:745
  130.6 1.5 %copy.18 = bf16[256,128]{1,0:T(8,128)(2,1)} copy(bf16[256,128]{1,0:T(8,128)(2,1)} %shard_map.154) | data formatting | bytes 131072

commit v2 on v1

--- a/solution.py
+++ b/solution.py
@@ -68,11 +68,28 @@
 def semaphore_count(nz, nc, tp):
     blocks = nz * nc
     chunks = max(1, nz // CHUNK)
-    return 1 + 3 + 3 + 1 + 2 * blocks + (chunks * 32 + 16 if tp > 1 else 0)
+    return 1 + 3 + 3 + 1 + 2 * blocks + (chunks * 28 + 12 if tp > 1 else 0)
 
 
 def kernel(
     sizes,
+    asker_hbm,
+    retain_hbm,
+    entries_hbm,
+    emit_hbm,
+    least_hbm,
+    extra_hbm,
+    lane_gain_hbm,
+    row_gain_hbm,
+    ids_hbm,
+    chance_hbm,
+    duo_hbm,
+    skip_hbm,
+    project_hbm,
+    switch_hbm,
+    raise_hbm,
+    lower_hbm,
+    out,
     asker,
     retain,
     entries,
@@ -84,12 +101,6 @@
     ids,
     chance,
     duo,
-    skip_hbm,
-    project_hbm,
-    switch_hbm,
-    raise_hbm,
-    lower_hbm,
-    out,
     skip,
     project,
     switch,
@@ -112,10 +123,8 @@
     route,
     mix_part,
     mix_one,
-    mix_two,
     mix_sum,
     mix_three,
-    mix_four,
     slots,
     rows,
     normed,
@@ -124,7 +133,6 @@
     red_two,
     red_sum,
     red_three,
-    red_four,
     finished,
     returned,
     local_sems,
@@ -153,7 +161,7 @@
     barrier = pltpu.get_barrier_semaphore()
     peers = [device(dz=dz, dc=dc) for dz in steps for dc in range(nc) if (dz, dc) != (0, 0)]
     if tp > 1:
-        peers += [device(dy=1), device(dy=-1), device(dx=1), device(dx=-1)]
+        peers += [device(dy=d) for d in (1, -1, 2)] + [device(dx=d) for d in (1, -1, 2)]
     for peer in peers:
         pl.semaphore_signal(barrier, inc=1, device_id=peer, device_id_type=MESH)
 
@@ -162,8 +170,19 @@
         pltpu.make_async_copy(src, dst, local_sems.at[i])
         for i, (src, dst) in enumerate(
             [
+                (retain_hbm, retain),
+                (least_hbm, least),
+                (extra_hbm, extra),
+                (entries_hbm, entries),
+                (asker_hbm, asker),
+                (emit_hbm, emit),
+                (lane_gain_hbm, lane_gain),
+                (ids_hbm, ids),
+                (chance_hbm, chance),
+                (duo_hbm, duo),
                 (project_hbm, project),
                 (skip_hbm.at[:, my_cols], skip),
+                (row_gain_hbm, row_gain),
                 (switch_hbm, switch),
                 (raise_hbm, raised),
                 (lower_hbm, lower),
@@ -172,6 +191,8 @@
     ]
     for load in loads:
         load.start()
+    for load in loads[:4]:
+        load.wait()
 
     spots = lax.broadcasted_iota(jnp.int32, (half, half), 0)
     other = lax.broadcasted_iota(jnp.int32, (half, half), 1)
@@ -222,6 +243,8 @@
 
     pl.semaphore_wait(barrier, len(peers))
 
+    for load in loads[4:10]:
+        load.wait()
     n_half = wire.slots(1)
     n_near = wire.slots(3)
     n_far = wire.slots(3)
@@ -339,7 +362,7 @@
             wire.copy(far.at[group], far.at[group], n_far + j - 1, to_group(j)).wait_send()
 
     second = jnp.exp(lasts[0]) * carried + state_first[...]
-    loads[0].wait()
+    loads[10].wait()
     for b, state in enumerate((carried, second)):
         mine = pl.ds(b * half, half)
         readout = inside[mine, :] + dims_of(query_hat[mine, :], state, 1, 1, HIGH)
@@ -356,11 +379,14 @@
                     .astype(BF)
                 )
 
+    ways = (2, 1, -1)
+
     class Reduce:
-        def __init__(self, source, lo, n, one, two, total, three, four):
-            self.source, self.lo, self.n = source, lo, n
-            self.bufs = (one, two, total, three, four)
-            self.first = wire.slots(16)
+        def __init__(self, source, lo, n, direct, one, two, total, three):
+            self.source, self.lo, self.n, self.direct = source, lo, n, direct
+            self.one, self.two, self.total, self.three = one, two, total, three
+            self.each = 6 if direct else 7
+            self.first = wire.slots(2 * self.each)
 
         def at(self, k, f, g):
             rest = (k, pl.ds(self.lo, self.n))
@@ -371,101 +397,87 @@
             name_f, name_g = ("dy", "dx") if k == 0 else ("dx", "dy")
             return f, g, (lambda d: device(**{name_f: d})), (lambda d: device(**{name_g: d}))
 
-        def number(self, k, step, way):
-            return self.first + k * 8 + step * 2 + way
+        def number(self, k, i):
+            return self.first + k * self.each + i
 
         def step_one(self):
-            one = self.bufs[0]
             for k in range(2):
                 f, g, to_f, to_g = self.axes(k)
+                if self.direct:
+                    for way, delta in enumerate(ways):
+                        wire.send(
+                            self.at(k, lax.rem(f + delta + 4, 4), pl.ds(0, 4)),
+                            self.one.at[k, way],
+                            self.number(k, way),
+                            to_f(delta),
+                        )
+                    continue
                 across = lax.rem(f + 2, 4)
                 for way, delta in ((0, 1), (1, -1)):
                     wire.send(
                         self.at(k, across, pl.ds(2 * way, 2)),
-                        one.at[k, way],
-                        self.number(k, 0, way),
+                        self.one.at[k, way],
+                        self.number(k, way),
                         to_f(delta),
                     )
 
         def step_two(self):
-            one, two = self.bufs[0], self.bufs[1]
             for k in range(2):
                 f, g, to_f, to_g = self.axes(k)
                 for way, delta in ((0, 1), (1, -1)):
-                    wire.arrived(one.at[k, way], self.number(k, 0, way), to_f(-delta))
+                    wire.arrived(self.one.at[k, way], self.number(k, way), to_f(-delta))
                     mine = self.at(k, lax.rem(f + delta + 4, 4), pl.ds(2 * way, 2))
-                    mine[...] = (mine[...].astype(F32) + one[k, way].astype(F32)).astype(BF)
+                    mine[...] = (mine[...].astype(F32) + self.one[k, way].astype(F32)).astype(BF)
             for k in range(2):
                 f, g, to_f, to_g = self.axes(k)
                 for way, delta in ((0, 1), (1, -1)):
                     wire.send(
                         self.at(k, lax.rem(f + delta + 4, 4), pl.ds(0, 4)),
-                        two.at[k, way],
-                        self.number(k, 1, way),
+                        self.two.at[k, way],
+                        self.number(k, 2 + way),
                         to_f(delta),
                     )
 
+        def inner(self):
+            if self.direct:
+                return [(self.one, way, delta, way) for way, delta in enumerate(ways)]
+            return [(self.two, way, delta, 2 + way) for way, delta in ((0, 1), (1, -1))]
+
         def step_three(self):
-            two, total, three = self.bufs[1], self.bufs[2], self.bufs[3]
-            h = self.n // 2
             for k in range(2):
                 f, g, to_f, to_g = self.axes(k)
-                for way, delta in ((0, 1), (1, -1)):
-                    wire.arrived(two.at[k, way], self.number(k, 1, way), to_f(-delta))
-                total[k] = (
-                    self.at(k, f, pl.ds(0, 4))[...].astype(F32)
-                    + two[k, 0].astype(F32)
-                    + two[k, 1].astype(F32)
-                ).astype(BF)
+                value = self.at(k, f, pl.ds(0, 4))[...].astype(F32)
+                for buf, way, delta, i in self.inner():
+                    wire.arrived(buf.at[k, way], self.number(k, i), to_f(-delta))
+                    value = value + buf[k, way].astype(F32)
+                self.total[k] = value.astype(BF)
             for k in range(2):
                 f, g, to_f, to_g = self.axes(k)
-                for way, delta in ((0, 1), (1, -1)):
+                for way, delta in enumerate(ways):
                     wire.send(
-                        total.at[k, lax.rem(g + 2, 4), pl.ds(way * h, h)],
-                        three.at[k, way],
-                        self.number(k, 2, way),
+                        self.total.at[k, lax.rem(g + delta + 4, 4)],
+                        self.three.at[k, way],
+                        self.number(k, self.each - 3 + way),
                         to_g(delta),
                     )
 
-        def step_four(self):
-            total, three, four = self.bufs[2], self.bufs[3], self.bufs[4]
-            h = self.n // 2
-            for k in range(2):
-                f, g, to_f, to_g = self.axes(k)
-                for way, delta in ((0, 1), (1, -1)):
-                    wire.arrived(three.at[k, way], self.number(k, 2, way), to_g(-delta))
-                    mine = total.at[k, lax.rem(g + delta + 4, 4), pl.ds(way * h, h)]
-                    mine[...] = (mine[...].astype(F32) + three[k, way].astype(F32)).astype(BF)
-            for k in range(2):
-                f, g, to_f, to_g = self.axes(k)
-                for way, delta in ((0, 1), (1, -1)):
-                    wire.send(
-                        total.at[k, lax.rem(g + delta + 4, 4)],
-                        four.at[k, way],
-                        self.number(k, 3, way),
-                        to_g(delta),
-                    )
-
         def result(self, k):
-            two, four = self.bufs[1], self.bufs[4]
             f, g, to_f, to_g = self.axes(k)
-            for way, delta in ((0, 1), (1, -1)):
-                wire.arrived(four.at[k, way], self.number(k, 3, way), to_g(-delta))
-            return (
-                self.at(k, f, g)[...].astype(F32)
-                + two[k, 0, g].astype(F32)
-                + two[k, 1, g].astype(F32)
-                + four[k, 0].astype(F32)
-                + four[k, 1].astype(F32)
-            )
-
-    loads[1].wait()
+            value = self.at(k, f, g)[...].astype(F32)
+            for buf, way, delta, i in self.inner():
+                value = value + buf[k, way, g].astype(F32)
+            for way, delta in enumerate(ways):
+                wire.arrived(
+                    self.three.at[k, way], self.number(k, self.each - 3 + way), to_g(-delta)
+                )
+                value = value + self.three[k, way].astype(F32)
+            return value
+
+    loads[11].wait()
     if tp > 1:
-        mix = Reduce(mix_part, 0, 2, mix_one, mix_two, mix_sum, mix_three, mix_four)
+        mix = Reduce(mix_part, 0, 2, True, mix_one, None, mix_sum, mix_three)
         mix.step_one()
-        mix.step_two()
         mix.step_three()
-        mix.step_four()
         own_cols = [mix.result(k).reshape(half, 128) for k in range(2)]
     else:
         own_cols = [mix_part[0, 0, k].astype(F32).reshape(half, 128) for k in range(2)]
@@ -498,12 +510,13 @@
             self.lo = number * CHUNK
             self.number = number
             if tp > 1:
-                self.first = wire.slots(16)
+                self.first = wire.slots(14)
                 self.red = Reduce(
                     part,
                     self.lo,
                     CHUNK,
-                    *(b.at[number] for b in (red_one, red_two, red_sum, red_three, red_four)),
+                    False,
+                    *(b.at[number] for b in (red_one, red_two, red_sum, red_three)),
                 )
 
         def at(self, k, p, s, lo=0, n=CHUNK):
@@ -515,8 +528,8 @@
             name_p, name_s = ("dx", "dy") if k == 0 else ("dy", "dx")
             return p, s, (lambda d: device(**{name_p: d})), (lambda d: device(**{name_s: d}))
 
-        def sem(self, k, step, way):
-            return self.first + k * 8 + step * 2 + way
+        def sem(self, k, i):
+            return self.first + k * 7 + i
 
         def gather_one(self):
             for i in range(self.lo, self.lo + CHUNK):
@@ -529,43 +542,28 @@
                 return
             for k in range(2):
                 p, s, to_p, to_s = self.axes(k)
-                for way, delta in ((0, 1), (1, -1)):
-                    mine = self.at(k, p, s)
-                    wire.send(mine, mine, self.sem(k, 0, way), to_p(delta))
+                mine = self.at(k, p, s)
+                for way, delta in enumerate(ways):
+                    wire.send(mine, mine, self.sem(k, way), to_p(delta))
 
         def gather_two(self):
-            h = CHUNK // 2
             for k in range(2 if tp > 1 else 0):
                 p, s, to_p, to_s = self.axes(k)
-                for way, delta in ((0, 1), (1, -1)):
+                for way, delta in enumerate(ways):
                     came = lax.rem(p - delta + 4, 4)
-                    wire.arrived(self.at(k, came, s), self.sem(k, 0, way), to_p(-delta))
-                    onward = self.at(k, came, s, way * h, h)
-                    wire.send(onward, onward, self.sem(k, 1, way), to_p(delta))
-
-        def gather_three(self):
-            h = CHUNK // 2
-            for k in range(2 if tp > 1 else 0):
-                p, s, to_p, to_s = self.axes(k)
-                across = lax.rem(p + 2, 4)
-                for way, delta in ((0, 1), (1, -1)):
-                    wire.arrived(
-                        self.at(k, across, s, way * h, h), self.sem(k, 1, way), to_p(-delta)
-                    )
+                    wire.arrived(self.at(k, came, s), self.sem(k, way), to_p(-delta))
                 mine = self.at(k, pl.ds(0, 4), s)
                 for way, delta in ((0, 1), (1, -1)):
-                    wire.send(mine, mine, self.sem(k, 2, way), to_s(delta))
-
-        def gather_four(self):
+                    wire.send(mine, mine, self.sem(k, 3 + way), to_s(delta))
+
+        def gather_three(self):
             for k in range(2 if tp > 1 else 0):
                 p, s, to_p, to_s = self.axes(k)
                 for way, delta in ((0, 1), (1, -1)):
                     came = lax.rem(s - delta + 4, 4)
-                    wire.arrived(
-                        self.at(k, pl.ds(0, 4), came), self.sem(k, 2, way), to_s(-delta)
-                    )
+                    wire.arrived(self.at(k, pl.ds(0, 4), came), self.sem(k, 3 + way), to_s(-delta))
                     onward = self.at(k, pl.ds(2 * way, 2), came)
-                    wire.send(onward, onward, self.sem(k, 3, way), to_s(delta))
+                    wire.send(onward, onward, self.sem(k, 5 + way), to_s(delta))
 
         def experts(self):
             for k in range(2 if tp > 1 else 0):
@@ -573,7 +571,7 @@
                 across = lax.rem(s + 2, 4)
                 for way, delta in ((0, 1), (1, -1)):
                     wire.arrived(
-                        self.at(k, pl.ds(2 * way, 2), across), self.sem(k, 3, way), to_s(-delta)
+                        self.at(k, pl.ds(2 * way, 2), across), self.sem(k, 5 + way), to_s(-delta)
                     )
             span = pl.ds(self.lo, CHUNK)
             count = nc * CHUNK * cap
@@ -610,10 +608,6 @@
             if tp > 1:
                 self.red.step_three()
 
-        def sum_four(self):
-            if tp > 1:
-                self.red.step_four()
-
         def give_back(self):
             for k in range(2):
                 if tp > 1:
@@ -635,20 +629,18 @@
 
     n_back_rows = wire.slots(nz * nc)
     work = [Chunk(n) for n in range(chunks)]
-    for load in loads[2:]:
+    for load in loads[12:]:
         load.wait()
     order = (
         "gather_one",
         "gather_two",
         "gather_three",
-        "gather_four",
         "experts",
         "sum_two",
         "sum_three",
-        "sum_four",
         "give_back",
     )
-    tasks = sorted((j + 2 * n, n, j) for n in range(chunks) for j in range(len(order)))
+    tasks = sorted((2 * j + n, n, j) for n in range(chunks) for j in range(len(order)))
     for _, n, j in tasks:
         getattr(work[n], order[j])()
 
@@ -702,6 +694,17 @@
     count = semaphore_count(nz, nc, tp)
     scratch = [
         pltpu.VMEM((tokens, 128), BF),
+        pltpu.VMEM((tokens, 128), BF),
+        pltpu.VMEM((tokens, 128), BF),
+        pltpu.VMEM((tokens, 128), BF),
+        pltpu.VMEM((1, 128), F32),
+        pltpu.VMEM((1, tokens), F32),
+        pltpu.VMEM((1, 128), F32),
+        pltpu.VMEM((1, width), F32),
+        pltpu.VMEM((2, tokens), jnp.int32),
+        pltpu.VMEM((1, tokens), F32),
+        pltpu.VMEM((2, tokens), F32),
+        pltpu.VMEM((tokens, 128), BF),
         pltpu.VMEM((128, width), BF),
         pltpu.VMEM((width, hidden), BF),
         pltpu.VMEM((width, hidden), BF),
@@ -722,11 +725,9 @@
         pltpu.VMEM((2, tokens, experts * cap), BF),
         pltpu.VMEM((2, tokens, 128), F32),
         pltpu.VMEM((ny, nx, 2, 2, half // 2, 128), BF),
-        pltpu.VMEM((2, 2, 2, 2, half // 2, 128), BF),
-        pltpu.VMEM((2, 2, 4, 2, half // 2, 128), BF),
+        pltpu.VMEM((2, 3, 4, 2, half // 2, 128), BF),
         pltpu.VMEM((2, 4, 2, half // 2, 128), BF),
-        pltpu.VMEM((2, 2, 1, half // 2, 128), BF),
-        pltpu.VMEM((2, 2, 2, half // 2, 128), BF),
+        pltpu.VMEM((2, 3, 2, half // 2, 128), BF),
         pltpu.VMEM((experts, *block), BF),
         pltpu.VMEM((ny, nx, nc, nz, *block), BF),
         pltpu.VMEM((nc * CHUNK * cap, width), BF),
@@ -734,18 +735,17 @@
         pltpu.VMEM((chunks, 2, 2, 2, CHUNK, *block), BF),
         pltpu.VMEM((chunks, 2, 2, 4, CHUNK, *block), BF),
         pltpu.VMEM((chunks, 2, 4, CHUNK, *block), BF),
-        pltpu.VMEM((chunks, 2, 2, CHUNK // 2, *block), BF),
-        pltpu.VMEM((chunks, 2, 2, CHUNK, *block), BF),
+        pltpu.VMEM((chunks, 2, 3, CHUNK, *block), BF),
         pltpu.VMEM((nc, nz, *block), BF),
         pltpu.VMEM((experts, *block), BF),
-        pltpu.SemaphoreType.DMA((5,)),
+        pltpu.SemaphoreType.DMA((16,)),
         pltpu.SemaphoreType.DMA((count,)),
         pltpu.SemaphoreType.DMA((count,)),
     ]
     return pl.pallas_call(
         functools.partial(kernel, sizes),
         out_shape=jax.ShapeDtypeStruct((tokens, 128), BF),
-        in_specs=[vmem] * 11 + [anywhere] * 5,
+        in_specs=[anywhere] * 16,
         out_specs=vmem,
         scratch_shapes=scratch,
         compiler_params=pltpu.CompilerParams(collective_id=0, has_side_effects=True),

time: 132 us -> 103 us (0.78)
  Pallas kernels: 131 us -> 102 us
    pallas_call x1, Pallas kernels: 131 us -> 102 us  [layer(): pl.pallas_call(functools.partial(kernel, sizes), out_shape=jax.ShapeDtype...]
where the time goes in v2:
time: 103 us
  Pallas kernels  102 us (99%)
  local copies, waits for them, and re-layouts  1.47 us (1%)
    pallas_call x1, Pallas kernels, layer(): pl.pallas_call(functools.partial(kernel, sizes), out_shape=jax.ShapeDtype...  102 us

profile of v2, /device:TPU:1, one launch (start us, length us, event | category | flops | bytes accessed | tf_op | source)
XLA Modules:
  0.0 103.3 jit_solution(15261090903691199423)
XLA Ops:
  0.0 101.8 %shard_map.154 = bf16[256,128]{1,0:T(8,128)(2,1)} custom-call(bf16[256,128]{1,0:T(8,128)(2,1)} %asker_hbm.1, bf16[256,128]{1,0:T(8,128)(2,1)} %retain_hbm.1, bf16[256,128]{1,0:T(8,128)(2,1)} %entries_hbm.1, bf16[256,128]{1,0:T(8,128)(2,1)} %emit_hbm.1, f32[1,128]{1,0:T(1,128)} %bitcast.16, f32[1,256]{1,0:T(1,128)} %extra_hbm.1, f32[1,128]{1,0:T(1,128)} %bitcast.17, ...), custom_call_target="tpu_custom_call" | custom-call | tf_op jit(solution)/shard_map/pallas_call | solution.py:745
  101.8 1.5 %copy.18 = bf16[256,128]{1,0:T(8,128)(2,1)} copy(bf16[256,128]{1,0:T(8,128)(2,1)} %shard_map.154) | data formatting | bytes 131072

commit v3 on v2

--- a/solution.py
+++ b/solution.py
@@ -16,8 +16,8 @@
 F32 = jnp.float32
 HIGH = lax.Precision.HIGHEST
 MESH = pl.DeviceIdType.MESH
+TILE = 8
 CHUNK = 4
-TILE = 8
 
 
 def dims_of(a, b, left, right, precision=None):
@@ -66,9 +66,7 @@
 
 
 def semaphore_count(nz, nc, tp):
-    blocks = nz * nc
-    chunks = max(1, nz // CHUNK)
-    return 1 + 3 + 3 + 1 + 2 * blocks + (chunks * 28 + 12 if tp > 1 else 0)
+    return 1 + 3 + 3 + 1 + 6 + 12 + 2 * nz + 26 * (nz // CHUNK)
 
 
 def kernel(
@@ -126,13 +124,17 @@
     mix_sum,
     mix_three,
     slots,
+    bands,
     rows,
     normed,
     part,
+    other_part,
+    summed,
     red_one,
-    red_two,
-    red_sum,
-    red_three,
+    red_a,
+    red_b,
+    last_a,
+    last_b,
     finished,
     returned,
     local_sems,
@@ -148,6 +150,8 @@
     wire = Wire(sends, recvs)
     steps = z_steps(nz)
     chunks = nz // CHUNK
+    mine_expert = lax.rem(x, 2)
+    keeps = c == mine_expert
 
     def device(dz=0, dc=0, dy=0, dx=0):
         return (
@@ -159,9 +163,9 @@
 
     partner = device(dc=1)
     barrier = pltpu.get_barrier_semaphore()
-    peers = [device(dz=dz, dc=dc) for dz in steps for dc in range(nc) if (dz, dc) != (0, 0)]
-    if tp > 1:
-        peers += [device(dy=d) for d in (1, -1, 2)] + [device(dx=d) for d in (1, -1, 2)]
+    peers = [partner] + [device(dz=dz) for dz in steps[1:]]
+    peers += [device(dy=d) for d in (1, -1, 2)] + [device(dx=d) for d in (1, -1, 2)]
+    peers += [device(dx=d, dc=1) for d in (1, -1)]
     for peer in peers:
         pl.semaphore_signal(barrier, inc=1, device_id=peer, device_id_type=MESH)
 
@@ -183,14 +187,23 @@
                 (project_hbm, project),
                 (skip_hbm.at[:, my_cols], skip),
                 (row_gain_hbm, row_gain),
-                (switch_hbm, switch),
-                (raise_hbm, raised),
-                (lower_hbm, lower),
             ]
         )
     ]
     for load in loads:
         load.start()
+    own_weights = [
+        pltpu.make_async_copy(src, dst, local_sems.at[13 + i])
+        for i, (src, dst) in enumerate(
+            [(switch_hbm, switch), (raise_hbm, raised), (lower_hbm, lower)]
+        )
+    ]
+
+    @pl.when(keeps)
+    def _():
+        for load in own_weights:
+            load.start()
+
     for load in loads[:4]:
         load.wait()
 
@@ -250,6 +263,29 @@
     n_far = wire.slots(3)
     n_back = wire.slots(1)
     wire.send(half_out, half_in, n_half, partner)
+
+    n_weights = wire.slots(6)
+    part_width = switch.shape[1] // 2
+
+    def moved(way, delta):
+        cut = slice(way * part_width, (way + 1) * part_width)
+        refs = [
+            (switch_hbm.at[:, cut], switch.at[:, cut]),
+            (raise_hbm.at[:, cut], raised.at[:, cut]),
+            (lower_hbm.at[cut, :], lower.at[cut, :]),
+        ]
+        there = device(dx=delta, dc=1)
+        return [
+            wire.copy(src, dst, n_weights + 3 * way + i, there) for i, (src, dst) in enumerate(refs)
+        ]
+
+    moves = moved(0, 1) + moved(1, -1)
+
+    @pl.when(jnp.logical_not(keeps))
+    def _():
+        for copy in moves:
+            copy.start()
+
 
     def score_block(b):
         total, keys = kept[b]
@@ -382,14 +418,14 @@
     ways = (2, 1, -1)
 
     class Reduce:
-        def __init__(self, source, lo, n, direct, one, two, total, three):
-            self.source, self.lo, self.n, self.direct = source, lo, n, direct
-            self.one, self.two, self.total, self.three = one, two, total, three
-            self.each = 6 if direct else 7
-            self.first = wire.slots(2 * self.each)
+        def __init__(self, source, lo, n, one, total, three):
+            self.source, self.one, self.total, self.three = source, one, total, three
+            self.first = wire.slots(12)
+            self.span = pl.ds(lo, n)
+            self.every = pl.ds(0, 4)
 
         def at(self, k, f, g):
-            rest = (k, pl.ds(self.lo, self.n))
+            rest = (k, self.span)
             return self.source.at[(f, g) + rest] if k == 0 else self.source.at[(g, f) + rest]
 
         def axes(self, k):
@@ -397,85 +433,50 @@
             name_f, name_g = ("dy", "dx") if k == 0 else ("dx", "dy")
             return f, g, (lambda d: device(**{name_f: d})), (lambda d: device(**{name_g: d}))
 
-        def number(self, k, i):
-            return self.first + k * self.each + i
-
         def step_one(self):
-            for k in range(2):
-                f, g, to_f, to_g = self.axes(k)
-                if self.direct:
-                    for way, delta in enumerate(ways):
-                        wire.send(
-                            self.at(k, lax.rem(f + delta + 4, 4), pl.ds(0, 4)),
-                            self.one.at[k, way],
-                            self.number(k, way),
-                            to_f(delta),
-                        )
-                    continue
-                across = lax.rem(f + 2, 4)
-                for way, delta in ((0, 1), (1, -1)):
-                    wire.send(
-                        self.at(k, across, pl.ds(2 * way, 2)),
-                        self.one.at[k, way],
-                        self.number(k, way),
-                        to_f(delta),
-                    )
-
-        def step_two(self):
-            for k in range(2):
-                f, g, to_f, to_g = self.axes(k)
-                for way, delta in ((0, 1), (1, -1)):
-                    wire.arrived(self.one.at[k, way], self.number(k, way), to_f(-delta))
-                    mine = self.at(k, lax.rem(f + delta + 4, 4), pl.ds(2 * way, 2))
-                    mine[...] = (mine[...].astype(F32) + self.one[k, way].astype(F32)).astype(BF)
-            for k in range(2):
-                f, g, to_f, to_g = self.axes(k)
-                for way, delta in ((0, 1), (1, -1)):
-                    wire.send(
-                        self.at(k, lax.rem(f + delta + 4, 4), pl.ds(0, 4)),
-                        self.two.at[k, way],
-                        self.number(k, 2 + way),
-                        to_f(delta),
-                    )
-
-        def inner(self):
-            if self.direct:
-                return [(self.one, way, delta, way) for way, delta in enumerate(ways)]
-            return [(self.two, way, delta, 2 + way) for way, delta in ((0, 1), (1, -1))]
-
-        def step_three(self):
-            for k in range(2):
-                f, g, to_f, to_g = self.axes(k)
-                value = self.at(k, f, pl.ds(0, 4))[...].astype(F32)
-                for buf, way, delta, i in self.inner():
-                    wire.arrived(buf.at[k, way], self.number(k, i), to_f(-delta))
-                    value = value + buf[k, way].astype(F32)
-                self.total[k] = value.astype(BF)
             for k in range(2):
                 f, g, to_f, to_g = self.axes(k)
                 for way, delta in enumerate(ways):
                     wire.send(
-                        self.total.at[k, lax.rem(g + delta + 4, 4)],
-                        self.three.at[k, way],
-                        self.number(k, self.each - 3 + way),
+                        self.at(k, lax.rem(f + delta + 4, 4), self.every),
+                        self.one.at[k, way, self.every, self.span],
+                        self.first + k * 6 + way,
+                        to_f(delta),
+                    )
+
+        def step_three(self):
+            for k in range(2):
+                f, g, to_f, to_g = self.axes(k)
+                value = self.at(k, f, self.every)[...].astype(F32)
+                for way, delta in enumerate(ways):
+                    came = self.one.at[k, way, self.every, self.span]
+                    wire.arrived(came, self.first + k * 6 + way, to_f(-delta))
+                    value = value + came[...].astype(F32)
+                self.total[k, self.every, self.span] = value.astype(BF)
+            for k in range(2):
+                f, g, to_f, to_g = self.axes(k)
+                for way, delta in enumerate(ways):
+                    wire.send(
+                        self.total.at[k, lax.rem(g + delta + 4, 4), self.span],
+                        self.three.at[k, way, self.span],
+                        self.first + k * 6 + 3 + way,
                         to_g(delta),
                     )
 
         def result(self, k):
             f, g, to_f, to_g = self.axes(k)
             value = self.at(k, f, g)[...].astype(F32)
-            for buf, way, delta, i in self.inner():
-                value = value + buf[k, way, g].astype(F32)
-            for way, delta in enumerate(ways):
-                wire.arrived(
-                    self.three.at[k, way], self.number(k, self.each - 3 + way), to_g(-delta)
-                )
-                value = value + self.three[k, way].astype(F32)
+            for way, delta in enumerate(ways):
+                value = value + self.one[k, way, g, self.span].astype(F32)
+            for way, delta in enumerate(ways):
+                came = self.three.at[k, way, self.span]
+                wire.arrived(came, self.first + k * 6 + 3 + way, to_g(-delta))
+                value = value + came[...].astype(F32)
             return value
 
     loads[11].wait()
     if tp > 1:
-        mix = Reduce(mix_part, 0, 2, True, mix_one, None, mix_sum, mix_three)
+        mix = Reduce(mix_part, 0, 2, mix_one, mix_sum, mix_three)
         mix.step_one()
         mix.step_three()
         own_cols = [mix.result(k).reshape(half, 128) for k in range(2)]
@@ -491,97 +492,90 @@
         .reshape(experts, tiles, TILE, 128)
         .astype(BF)
     )
-    rows[y, x, 0, 0] = slots[me_sp]
-    n_out = wire.slots(nz * nc)
+    n_out = wire.slots(nz)
+    bands[y, :, 0] = slots[pl.ds(2 * z, 2)]
     for i, dz in enumerate(steps):
-        for dc in range(nc):
-            if (dz, dc) == (0, 0):
-                continue
-            there = device(dz=dz, dc=dc)
-            wire.send(
-                slots.at[there[0] * nc + there[1]],
-                rows.at[y, x, dc, i],
-                n_out + i * nc + dc,
-                there,
-            )
+        if dz == 0:
+            continue
+        there = device(dz=dz)
+        wire.send(
+            slots.at[pl.ds(2 * there[0], 2)], bands.at[y, :, i], n_out + i, there
+        )
+
+    four = pl.ds(0, 4)
 
     class Chunk:
         def __init__(self, number):
             self.lo = number * CHUNK
-            self.number = number
-            if tp > 1:
-                self.first = wire.slots(14)
-                self.red = Reduce(
-                    part,
-                    self.lo,
-                    CHUNK,
-                    False,
-                    *(b.at[number] for b in (red_one, red_two, red_sum, red_three)),
-                )
-
-        def at(self, k, p, s, lo=0, n=CHUNK):
-            rest = (k, pl.ds(self.lo + lo, n))
-            return rows.at[(s, p) + rest] if k == 0 else rows.at[(p, s) + rest]
-
-        def axes(self, k):
-            p, s = (x, y) if k == 0 else (y, x)
-            name_p, name_s = ("dx", "dy") if k == 0 else ("dy", "dx")
-            return p, s, (lambda d: device(**{name_p: d})), (lambda d: device(**{name_s: d}))
-
-        def sem(self, k, i):
-            return self.first + k * 7 + i
+            self.h = CHUNK // 2
+            self.first = wire.slots(26)
+            self.whole = pl.ds(self.lo, CHUNK)
+            self.spans = [pl.ds(self.lo, self.h), pl.ds(self.lo + self.h, self.h)]
+
+        def expert_for(self, delta):
+            return mine_expert if delta == 2 else 1 - mine_expert
 
         def gather_one(self):
             for i in range(self.lo, self.lo + CHUNK):
-                for dc in range(nc):
-                    if (steps[i], dc) != (0, 0):
-                        wire.arrived(
-                            rows.at[y, x, dc, i], n_out + i * nc + dc, device(dz=-steps[i], dc=dc)
-                        )
-            if tp == 1:
-                return
-            for k in range(2):
-                p, s, to_p, to_s = self.axes(k)
-                mine = self.at(k, p, s)
-                for way, delta in enumerate(ways):
-                    wire.send(mine, mine, self.sem(k, way), to_p(delta))
+                if steps[i] != 0:
+                    wire.arrived(bands.at[y, :, i], n_out + i, device(dz=-steps[i]))
+            a, b = self.spans
+            for way, delta in enumerate(ways):
+                wire.send(
+                    bands.at[y, self.expert_for(delta), a],
+                    rows.at[y, x, c, a],
+                    self.first + way,
+                    device(dx=delta),
+                )
+                both = bands.at[y, pl.ds(0, 2), b]
+                wire.send(both, both, self.first + 3 + way, device(dy=delta))
+            rows[y, x, c, a] = bands[y, mine_expert, a]
 
         def gather_two(self):
-            for k in range(2 if tp > 1 else 0):
-                p, s, to_p, to_s = self.axes(k)
-                for way, delta in enumerate(ways):
-                    came = lax.rem(p - delta + 4, 4)
-                    wire.arrived(self.at(k, came, s), self.sem(k, way), to_p(-delta))
-                mine = self.at(k, pl.ds(0, 4), s)
-                for way, delta in ((0, 1), (1, -1)):
-                    wire.send(mine, mine, self.sem(k, 3 + way), to_s(delta))
+            a, b = self.spans
+            for way, delta in enumerate(ways):
+                came_x = lax.rem(x - delta + 4, 4)
+                wire.arrived(rows.at[y, came_x, c, a], self.first + way, device(dx=-delta))
+            for way, delta in enumerate(ways):
+                quad = rows.at[y, four, c, a]
+                wire.send(quad, quad, self.first + 6 + way, device(dy=delta))
+            for way, delta in enumerate(ways):
+                came_y = lax.rem(y - delta + 4, 4)
+                wire.arrived(
+                    bands.at[came_y, pl.ds(0, 2), b], self.first + 3 + way, device(dy=-delta)
+                )
+            for way, delta in enumerate(ways):
+                wire.send(
+                    bands.at[four, self.expert_for(delta), b],
+                    rows.at[four, x, c, b],
+                    self.first + 9 + way,
+                    device(dx=delta),
+                )
+            rows[four, x, c, b] = bands[four, mine_expert, b]
 
         def gather_three(self):
-            for k in range(2 if tp > 1 else 0):
-                p, s, to_p, to_s = self.axes(k)
-                for way, delta in ((0, 1), (1, -1)):
-                    came = lax.rem(s - delta + 4, 4)
-                    wire.arrived(self.at(k, pl.ds(0, 4), came), self.sem(k, 3 + way), to_s(-delta))
-                    onward = self.at(k, pl.ds(2 * way, 2), came)
-                    wire.send(onward, onward, self.sem(k, 5 + way), to_s(delta))
+            a, b = self.spans
+            for way, delta in enumerate(ways):
+                came_x, came_y = lax.rem(x - delta + 4, 4), lax.rem(y - delta + 4, 4)
+                wire.arrived(
+                    rows.at[came_y, four, c, a], self.first + 6 + way, device(dy=-delta)
+                )
+                wire.arrived(
+                    rows.at[four, came_x, c, b], self.first + 9 + way, device(dx=-delta)
+                )
+            mine = rows.at[four, four, c, self.whole]
+            wire.send(mine, mine, self.first + 12, partner)
 
         def experts(self):
-            for k in range(2 if tp > 1 else 0):
-                p, s, to_p, to_s = self.axes(k)
-                across = lax.rem(s + 2, 4)
-                for way, delta in ((0, 1), (1, -1)):
-                    wire.arrived(
-                        self.at(k, pl.ds(2 * way, 2), across), self.sem(k, 5 + way), to_s(-delta)
-                    )
-            span = pl.ds(self.lo, CHUNK)
+            wire.arrived(rows.at[four, four, 1 - c, self.whole], self.first + 12, partner)
             count = nc * CHUNK * cap
             squares = jnp.zeros((count, 128), F32)
             for t in range(tp):
-                wide = rows[t // nx, t % nx, :, span].astype(F32).reshape(count, 128)
+                wide = rows[t // nx, t % nx, :, self.whole].astype(F32).reshape(count, 128)
                 squares = squares + wide * wide
             scale = lax.rsqrt(jnp.sum(squares, axis=1, keepdims=True) / (tp * 128) + EPS)
             for t in range(tp):
-                wide = rows[t // nx, t % nx, :, span].astype(F32).reshape(count, 128)
+                wide = rows[t // nx, t % nx, :, self.whole].astype(F32).reshape(count, 128)
                 cols = slice(t * 128, (t + 1) * 128)
                 normed[:, cols] = (wide * scale * row_gain[:, cols]).astype(BF)
             gate_acts = jnp.dot(normed[...], switch[...], preferred_element_type=F32)
@@ -591,53 +585,135 @@
                 wide = jnp.dot(
                     hidden, lower[:, t * 128 : (t + 2) * 128], preferred_element_type=F32
                 )
-                for u in range(t, min(t + 2, tp)):
-                    part[u // nx, u % nx, :, span] = (
+                for u in range(t, t + 2):
+                    part[u // nx, u % nx, :, self.whole] = (
                         wide[:, (u - t) * 128 : (u - t + 1) * 128]
                         .reshape(nc, CHUNK, tiles, TILE, 128)
                         .astype(BF)
                     )
-            if tp > 1:
-                self.red.step_one()
+            wire.send(
+                part.at[four, four, 1 - c, self.whole],
+                other_part.at[four, four, self.whole],
+                self.first + 13,
+                partner,
+            )
+
+        def sum_one(self):
+            came = other_part.at[four, four, self.whole]
+            wire.arrived(came, self.first + 13, partner)
+            for t in range(tp):
+                at = (t // nx, t % nx)
+                summed[at[0], at[1], self.whole] = (
+                    part[at[0], at[1], c, self.whole].astype(F32)
+                    + other_part[at[0], at[1], self.whole].astype(F32)
+                ).astype(BF)
+            a, b = self.spans
+            for way, delta in enumerate(ways):
+                to_y, to_x = lax.rem(y + delta + 4, 4), lax.rem(x + delta + 4, 4)
+                wire.send(
+                    summed.at[to_y, four, a],
+                    red_one.at[way, four, a],
+                    self.first + 14 + way,
+                    device(dy=delta),
+                )
+                wire.send(
+                    summed.at[four, to_x, b],
+                    red_one.at[way, four, b],
+                    self.first + 17 + way,
+                    device(dx=delta),
+                )
+
+        def first_sum(self, index):
+            a = self.spans[0]
+            value = summed[y, index, a].astype(F32)
+            for way in range(3):
+                value = value + red_one[way, index, a].astype(F32)
+            return value
+
+        def second_sums(self, index):
+            b = self.spans[1]
+            own = summed[index, x, b].astype(F32) + red_one[0, index, b].astype(F32)
+            return own, red_one[1, index, b].astype(F32) + red_one[2, index, b].astype(F32)
 
         def sum_two(self):
-            if tp > 1:
-                self.red.step_two()
-
-        def sum_three(self):
-            if tp > 1:
-                self.red.step_three()
+            a, b = self.spans
+            for way, delta in enumerate(ways):
+                wire.arrived(
+                    red_one.at[way, four, a], self.first + 14 + way, device(dy=-delta)
+                )
+                wire.arrived(
+                    red_one.at[way, four, b], self.first + 17 + way, device(dx=-delta)
+                )
+            red_a[four, a] = self.first_sum(four).astype(BF)
+            own, other = self.second_sums(four)
+            red_b[four, mine_expert, b] = own.astype(BF)
+            red_b[four, 1 - mine_expert, b] = other.astype(BF)
+            for way, delta in enumerate(ways):
+                to_y, to_x = lax.rem(y + delta + 4, 4), lax.rem(x + delta + 4, 4)
+                wire.send(
+                    red_a.at[to_x, a],
+                    last_a.at[way, a],
+                    self.first + 20 + way,
+                    device(dx=delta),
+                )
+                wire.send(
+                    red_b.at[to_y, pl.ds(0, 2), b],
+                    last_b.at[way, pl.ds(0, 2), b],
+                    self.first + 23 + way,
+                    device(dy=delta),
+                )
 
         def give_back(self):
-            for k in range(2):
-                if tp > 1:
-                    done = self.red.result(k).astype(BF)
-                else:
-                    done = part[0, 0, k, pl.ds(self.lo, CHUNK)]
-                finished[k, pl.ds(self.lo, CHUNK)] = done
+            a, b = self.spans
+            for way, delta in enumerate(ways):
+                wire.arrived(last_a.at[way, a], self.first + 20 + way, device(dx=-delta))
+                wire.arrived(
+                    last_b.at[way, pl.ds(0, 2), b], self.first + 23 + way, device(dy=-delta)
+                )
+            finished[mine_expert, a] = (
+                self.first_sum(x) + last_a[0, a].astype(F32)
+            ).astype(BF)
+            finished[1 - mine_expert, a] = (
+                last_a[1, a].astype(F32) + last_a[2, a].astype(F32)
+            ).astype(BF)
+            own, other = self.second_sums(y)
+            for expert, value in ((mine_expert, own), (1 - mine_expert, other)):
+                for way in range(3):
+                    value = value + last_b[way, expert, b].astype(F32)
+                finished[expert, b] = value.astype(BF)
             for i in range(self.lo, self.lo + CHUNK):
-                for dc in range(nc):
-                    if (steps[i], dc) == (0, 0):
-                        returned[me_sp] = finished[0, 0]
-                        continue
-                    wire.send(
-                        finished.at[dc, i],
-                        returned.at[me_sp],
-                        n_back_rows + i * nc + dc,
-                        device(dz=-steps[i], dc=dc),
-                    )
-
-    n_back_rows = wire.slots(nz * nc)
+                if steps[i] == 0:
+                    returned[pl.ds(2 * z, 2)] = finished[:, i]
+                    continue
+                wire.send(
+                    finished.at[pl.ds(0, 2), i],
+                    returned.at[pl.ds(2 * z, 2)],
+                    n_home + i,
+                    device(dz=-steps[i]),
+                )
+
+    n_home = wire.slots(nz)
     work = [Chunk(n) for n in range(chunks)]
-    for load in loads[12:]:
-        load.wait()
+    loads[12].wait()
+
+    @pl.when(keeps)
+    def _():
+        for load in own_weights:
+            load.wait()
+
+    @pl.when(jnp.logical_not(keeps))
+    def _():
+        for copy in moves:
+            copy.wait_send()
+            copy.wait_recv()
+
     order = (
         "gather_one",
         "gather_two",
         "gather_three",
         "experts",
+        "sum_one",
         "sum_two",
-        "sum_three",
         "give_back",
     )
     tasks = sorted((2 * j + n, n, j) for n in range(chunks) for j in range(len(order)))
@@ -645,13 +721,9 @@
         getattr(work[n], order[j])()
 
     for i, dz in enumerate(steps):
-        for dc in range(nc):
-            if (dz, dc) == (0, 0):
-                continue
-            there = device(dz=dz, dc=dc)
-            wire.arrived(
-                returned.at[there[0] * nc + there[1]], n_back_rows + i * nc + dc, there
-            )
+        if dz != 0:
+            there = device(dz=dz)
+            wire.arrived(returned.at[pl.ds(2 * there[0], 2)], n_home + i, there)
     got_rows = returned[...].astype(F32).reshape(experts * cap, 128).astype(BF)
     result = skip[...].astype(F32)
     for j in range(2):
@@ -685,7 +757,7 @@
     tp = ny * nx
     width = tp * 128
     hidden = specialist_switch_proj.shape[2]
-    half, experts, chunks, tiles = tokens // 2, nz * nc, nz // CHUNK, cap // TILE
+    half, experts, tiles = tokens // 2, nz * nc, cap // TILE
     block = (tiles, TILE, 128)
     vmem, anywhere = (
         pl.BlockSpec(memory_space=pltpu.VMEM),
@@ -729,14 +801,18 @@
         pltpu.VMEM((2, 4, 2, half // 2, 128), BF),
         pltpu.VMEM((2, 3, 2, half // 2, 128), BF),
         pltpu.VMEM((experts, *block), BF),
+        pltpu.VMEM((ny, 2, nz, *block), BF),
         pltpu.VMEM((ny, nx, nc, nz, *block), BF),
         pltpu.VMEM((nc * CHUNK * cap, width), BF),
         pltpu.VMEM((ny, nx, nc, nz, *block), BF),
-        pltpu.VMEM((chunks, 2, 2, 2, CHUNK, *block), BF),
-        pltpu.VMEM((chunks, 2, 2, 4, CHUNK, *block), BF),
-        pltpu.VMEM((chunks, 2, 4, CHUNK, *block), BF),
-        pltpu.VMEM((chunks, 2, 3, CHUNK, *block), BF),
-        pltpu.VMEM((nc, nz, *block), BF),
+        pltpu.VMEM((ny, nx, nz, *block), BF),
+        pltpu.VMEM((ny, nx, nz, *block), BF),
+        pltpu.VMEM((3, 4, nz, *block), BF),
+        pltpu.VMEM((4, nz, *block), BF),
+        pltpu.VMEM((4, 2, nz, *block), BF),
+        pltpu.VMEM((3, nz, *block), BF),
+        pltpu.VMEM((3, 2, nz, *block), BF),
+        pltpu.VMEM((2, nz, *block), BF),
         pltpu.VMEM((experts, *block), BF),
         pltpu.SemaphoreType.DMA((16,)),
         pltpu.SemaphoreType.DMA((count,)),

time: 103 us -> 98.3 us (0.954); the launches traced: 103 us -> 97.4 us
  Pallas kernels: 102 us -> 95.9 us
    pallas_call x1, Pallas kernels: 102 us -> 95.9 us  [layer(): pl.pallas_call(functools.partial(kernel, sizes), out_shape=jax.ShapeDtype...]
where the time goes in v3:
time: 98.3 us; the launch traced here: 97.4 us
  Pallas kernels  95.9 us (98%)
  local copies, waits for them, and re-layouts  1.47 us (1%)
    pallas_call x1, Pallas kernels, layer(): pl.pallas_call(functools.partial(kernel, sizes), out_shape=jax.ShapeDtype...  95.9 us

profile of v3, /device:TPU:1, one launch (start us, length us, event | category | flops | bytes accessed | tf_op | source)
XLA Modules:
  0.0 97.4 jit_solution(14616132177204873073)
XLA Ops:
  0.0 95.9 %shard_map.154 = bf16[256,128]{1,0:T(8,128)(2,1)} custom-call(bf16[256,128]{1,0:T(8,128)(2,1)} %asker_hbm.1, bf16[256,128]{1,0:T(8,128)(2,1)} %retain_hbm.1, bf16[256,128]{1,0:T(8,128)(2,1)} %entries_hbm.1, bf16[256,128]{1,0:T(8,128)(2,1)} %emit_hbm.1, f32[1,128]{1,0:T(1,128)} %bitcast.16, f32[1,256]{1,0:T(1,128)} %extra_hbm.1, f32[1,128]{1,0:T(1,128)} %bitcast.17, ...), custom_call_target="tpu_custom_call" | custom-call | tf_op jit(solution)/shard_map/pallas_call | solution.py:821
  95.9 1.5 %copy.18 = bf16[256,128]{1,0:T(8,128)(2,1)} copy(bf16[256,128]{1,0:T(8,128)(2,1)} %shard_map.154) | data formatting | bytes 131072

commit v4 on v3

--- a/solution.py
+++ b/solution.py
@@ -30,7 +30,8 @@
     steps = [0]
     for far in range(1, count // 2 + 1):
         steps += [far, -far]
-    return steps[:count]
+    steps = steps[:count]
+    return steps[4:] + steps[:4] if count > 4 else steps
 
 
 def column_of(row, eye):
@@ -104,6 +105,9 @@
     switch,
     raised,
     lower,
+    away_switch,
+    away_raised,
+    away_lower,
     state_own,
     state_first,
     half_out,
@@ -163,7 +167,7 @@
 
     partner = device(dc=1)
     barrier = pltpu.get_barrier_semaphore()
-    peers = [partner] + [device(dz=dz) for dz in steps[1:]]
+    peers = [partner] + [device(dz=dz) for dz in steps if dz != 0]
     peers += [device(dy=d) for d in (1, -1, 2)] + [device(dx=d) for d in (1, -1, 2)]
     peers += [device(dx=d, dc=1) for d in (1, -1)]
     for peer in peers:
@@ -199,9 +203,21 @@
         )
     ]
 
+    staged = [
+        pltpu.make_async_copy(src, dst, local_sems.at[16 + i])
+        for i, (src, dst) in enumerate(
+            [(switch_hbm, away_switch), (raise_hbm, away_raised), (lower_hbm, away_lower)]
+        )
+    ]
+
     @pl.when(keeps)
     def _():
         for load in own_weights:
+            load.start()
+
+    @pl.when(jnp.logical_not(keeps))
+    def _():
+        for load in staged:
             load.start()
 
     for load in loads[:4]:
@@ -270,20 +286,23 @@
     def moved(way, delta):
         cut = slice(way * part_width, (way + 1) * part_width)
         refs = [
-            (switch_hbm.at[:, cut], switch.at[:, cut]),
-            (raise_hbm.at[:, cut], raised.at[:, cut]),
-            (lower_hbm.at[cut, :], lower.at[cut, :]),
+            (away_switch.at[:, cut], switch.at[:, cut]),
+            (away_raised.at[:, cut], raised.at[:, cut]),
+            (away_lower.at[cut, :], lower.at[cut, :]),
         ]
         there = device(dx=delta, dc=1)
         return [
             wire.copy(src, dst, n_weights + 3 * way + i, there) for i, (src, dst) in enumerate(refs)
         ]
 
-    moves = moved(0, 1) + moved(1, -1)
+    right_ones, left_ones = moved(0, 1), moved(1, -1)
+    early, late = right_ones[:2] + left_ones[:2], [right_ones[2], left_ones[2]]
 
     @pl.when(jnp.logical_not(keeps))
     def _():
-        for copy in moves:
+        for load in staged:
+            load.wait()
+        for copy in early:
             copy.start()
 
 
@@ -486,6 +505,11 @@
         mine = pl.ds(k * half, half)
         skip[mine, :] = (skip[mine, :].astype(F32) + own_cols[k]).astype(BF)
 
+    @pl.when(jnp.logical_not(keeps))
+    def _():
+        for copy in late:
+            copy.start()
+
     tiles = cap // TILE
     slots[...] = (
         jnp.dot(select_in[...], skip[...], preferred_element_type=F32)
@@ -493,7 +517,7 @@
         .astype(BF)
     )
     n_out = wire.slots(nz)
-    bands[y, :, 0] = slots[pl.ds(2 * z, 2)]
+    bands[y, :, steps.index(0)] = slots[pl.ds(2 * z, 2)]
     for i, dz in enumerate(steps):
         if dz == 0:
             continue
@@ -568,6 +592,8 @@
 
         def experts(self):
             wire.arrived(rows.at[four, four, 1 - c, self.whole], self.first + 12, partner)
+            if self.lo == 0:
+                weights_are_here()
             count = nc * CHUNK * cap
             squares = jnp.zeros((count, 128), F32)
             for t in range(tp):
@@ -696,16 +722,17 @@
     work = [Chunk(n) for n in range(chunks)]
     loads[12].wait()
 
-    @pl.when(keeps)
-    def _():
-        for load in own_weights:
-            load.wait()
-
-    @pl.when(jnp.logical_not(keeps))
-    def _():
-        for copy in moves:
-            copy.wait_send()
-            copy.wait_recv()
+    def weights_are_here():
+        @pl.when(keeps)
+        def _():
+            for load in own_weights:
+                load.wait()
+
+        @pl.when(jnp.logical_not(keeps))
+        def _():
+            for copy in early + late:
+                copy.wait_send()
+                copy.wait_recv()
 
     order = (
         "gather_one",
@@ -716,7 +743,8 @@
         "sum_two",
         "give_back",
     )
-    tasks = sorted((2 * j + n, n, j) for n in range(chunks) for j in range(len(order)))
+    at = (0, 3, 7, 9, 11, 15, 19)
+    tasks = sorted((at[j] + 2.2 * n, n, j) for n in range(chunks) for j in range(len(order)))
     for _, n, j in tasks:
         getattr(work[n], order[j])()
 
@@ -781,6 +809,9 @@
         pltpu.VMEM((width, hidden), BF),
         pltpu.VMEM((width, hidden), BF),
         pltpu.VMEM((hidden, width), BF),
+        pltpu.VMEM((width, hidden), BF),
+        pltpu.VMEM((width, hidden), BF),
+        pltpu.VMEM((hidden, width), BF),
         pltpu.VMEM((128, 128), F32),
         pltpu.VMEM((128, 128), F32),
         pltpu.VMEM((80, 128), BF),
@@ -814,7 +845,7 @@
         pltpu.VMEM((3, 2, nz, *block), BF),
         pltpu.VMEM((2, nz, *block), BF),
         pltpu.VMEM((experts, *block), BF),
-        pltpu.SemaphoreType.DMA((16,)),
+        pltpu.SemaphoreType.DMA((19,)),
         pltpu.SemaphoreType.DMA((count,)),
         pltpu.SemaphoreType.DMA((count,)),
     ]

time: 98.3 us -> 94.3 us (0.959)
  Pallas kernels: 95.9 us -> 91.6 us
    pallas_call x1, Pallas kernels: 95.9 us -> 91.6 us  [layer(): pl.pallas_call(functools.partial(kernel, sizes), out_shape=jax.ShapeDtype...]
where the time goes in v4:
time: 94.3 us; the launch traced here: 93.1 us
  Pallas kernels  91.6 us (97%)
  local copies, waits for them, and re-layouts  1.47 us (2%)
    pallas_call x1, Pallas kernels, layer(): pl.pallas_call(functools.partial(kernel, sizes), out_shape=jax.ShapeDtype...  91.6 us

profile of v4, /device:TPU:1, one launch (start us, length us, event | category | flops | bytes accessed | tf_op | source)
XLA Modules:
  0.0 93.1 jit_solution(1074322311228835867)
XLA Ops:
  0.0 91.6 %shard_map.154 = bf16[256,128]{1,0:T(8,128)(2,1)} custom-call(bf16[256,128]{1,0:T(8,128)(2,1)} %asker_hbm.1, bf16[256,128]{1,0:T(8,128)(2,1)} %retain_hbm.1, bf16[256,128]{1,0:T(8,128)(2,1)} %entries_hbm.1, bf16[256,128]{1,0:T(8,128)(2,1)} %emit_hbm.1, f32[1,128]{1,0:T(1,128)} %bitcast.16, f32[1,256]{1,0:T(1,128)} %extra_hbm.1, f32[1,128]{1,0:T(1,128)} %bitcast.17, ...), custom_call_target="tpu_custom_call" | custom-call | tf_op jit(solution)/shard_map/pallas_call | solution.py:852
  91.6 1.5 %copy.18 = bf16[256,128]{1,0:T(8,128)(2,1)} copy(bf16[256,128]{1,0:T(8,128)(2,1)} %shard_map.154) | data formatting | bytes 131072

commit v5 on v4

--- a/solution.py
+++ b/solution.py
@@ -420,7 +420,7 @@
     loads[10].wait()
     for b, state in enumerate((carried, second)):
         mine = pl.ds(b * half, half)
-        readout = inside[mine, :] + dims_of(query_hat[mine, :], state, 1, 1, HIGH)
+        readout = inside[mine, :] + dims_of(query_hat[mine, :], state, 1, 1)
         mean = jnp.mean(readout * readout, axis=1, keepdims=True)
         mixed = (readout * lax.rsqrt(mean + EPS) * gates[mine, :]).astype(BF)
         for t in range(0, tp, 2):

time: 94.3 us -> 93.9 us (level)
  no operation moved by 1% of the time
where the time goes in v5:
time: 93.9 us; the launch traced here: 93.2 us
  Pallas kernels  91.7 us (98%)
  local copies, waits for them, and re-layouts  1.47 us (2%)
    pallas_call x1, Pallas kernels, layer(): pl.pallas_call(functools.partial(kernel, sizes), out_shape=jax.ShapeDtype...  91.7 us

profile of v5, /device:TPU:1, one launch (start us, length us, event | category | flops | bytes accessed | tf_op | source)
XLA Modules:
  0.0 93.2 jit_solution(11130539136371852471)
XLA Ops:
  0.0 91.7 %shard_map.154 = bf16[256,128]{1,0:T(8,128)(2,1)} custom-call(bf16[256,128]{1,0:T(8,128)(2,1)} %asker_hbm.1, bf16[256,128]{1,0:T(8,128)(2,1)} %retain_hbm.1, bf16[256,128]{1,0:T(8,128)(2,1)} %entries_hbm.1, bf16[256,128]{1,0:T(8,128)(2,1)} %emit_hbm.1, f32[1,128]{1,0:T(1,128)} %bitcast.16, f32[1,256]{1,0:T(1,128)} %extra_hbm.1, f32[1,128]{1,0:T(1,128)} %bitcast.17, ...), custom_call_target="tpu_custom_call" | custom-call | tf_op jit(solution)/shard_map/pallas_call | solution.py:852
  91.7 1.5 %copy.18 = bf16[256,128]{1,0:T(8,128)(2,1)} copy(bf16[256,128]{1,0:T(8,128)(2,1)} %shard_map.154) | data formatting | bytes 131072
